TPU v7x, 32 devices: a whole 2x2x4 slice. The times are simulated.
32 devices in a mesh: ep: 8 (over z, x), tp: 4 (over y, core).
Axes of the slice: x: 2, y: 2, z: 4, core: 2. Of those that a mesh axis runs over, the one named last changes fastest.
Arguments:
- residual_in: bfloat16 [128, 2048], P('ep'), may hold values from -6 to 6
- lengths: int32 [128], P('ep'), may hold values from 1 to 511, as said below
- kv_cache: bfloat16 [128, 4, 512, 256], P('ep', 'tp'), may hold values from -640 to 640
- norm_gain_attn: float32 [2048], replicated, may hold values from 0.1 to 1.9
- query_weight: bfloat16 [2048, 2048], P(None, 'tp'), may hold values from -0.125 to 0.125
- key_weight: bfloat16 [2048, 512], P(None, 'tp'), may hold values from -0.125 to 0.125
- value_weight: bfloat16 [2048, 512], P(None, 'tp'), may hold values from -0.125 to 0.125
- diff_lambda: float32 [16], P('tp'), may hold values from 0.3 to 0.8
- head_gain: float32 [128], replicated, may hold values from 0.1 to 1.9
- out_weight: bfloat16 [2048, 2048], P(None, 'tp'), may hold values from -0.125 to 0.125
- norm_gain_ffn: float32 [2048], replicated, may hold values from 0.1 to 1.9
- route_ids: int32 [128, 2], P('ep'), may hold values from 0 to 7, as said below
- route_weights: float32 [128, 2], P('ep'), may hold values from 0.1 to 1
- expert_gate: bfloat16 [8, 2048, 512], P('ep', None, 'tp'), may hold values from -0.125 to 0.125
- expert_up: bfloat16 [8, 2048, 512], P('ep', None, 'tp'), may hold values from -0.125 to 0.125
- expert_down: bfloat16 [8, 512, 2048], P('ep', 'tp'), may hold values from -0.25 to 0.25
- dense_gate: bfloat16 [2048, 8192], P(None, 'ep'), may hold values from -0.125 to 0.125
- dense_up: bfloat16 [2048, 8192], P(None, 'ep'), may hold values from -0.125 to 0.125
- dense_down: bfloat16 [8192, 2048], P('ep'), may hold values from -0.0625 to 0.0625
- dense_mix: float32 [2048], replicated, may hold values from -0.125 to 0.125
Outputs:
- layer_out: bfloat16 [128, 2048], P('ep', 'tp')
- new_rows: bfloat16 [128, 4, 256], P('ep', 'tp')
Inputs may be any that keep to these rules, and one draw needn't show every extreme that they name: The new token stands at position lengths[b]; some sequence holds 511 positions in every draw. `route_ids`: each row names 2 different experts from one group; the groups are the 4 runs of consecutive expert numbers of equal size. Among the rows of one index of ep no expert is named more than 8 times, and some expert exactly 8 times.
All inputs are finite; a program needn't handle non-finite values.
Results may differ from a plain program's by a relative error of at most 0.008.
The roundings to bfloat16 on the way count: a program that leaves them out, or rounds other values in their place, can miss the bound.
Values may be sent and summed in bfloat16 or wider, within the bound.
A program may use at most 64 MiB of HBM per device.

v0:
```python
import functools
import math

import jax
import jax.numpy as jnp
from jax import lax
from jax.experimental import pallas as pl
from jax.experimental.pallas import tpu as pltpu
from jax.sharding import PartitionSpec as P

QK_DIM = 64
EPS = 1e-06
MESH = pl.DeviceIdType.MESH
F32 = jnp.float32
BF16 = jnp.bfloat16
LANES = 128
Q_CHUNKS = 4


def flip(value, mask):
    bit = 1
    while bit <= mask:
        if mask & bit:
            value = value + bit * (1 - 2 * ((value // bit) % 2))
        bit *= 2
    return value


def each(count, body, order=None):
    if count <= 16:
        for index in order if order is not None else range(count):
            body(index)
    else:

        def step(index, carry):
            body(index)
            return carry

        lax.fori_loop(0, count, step, 0)


def block(start, size):
    return pl.ds(pl.multiple_of(start * size, size), size)


def remote(source, target, send, recv, where):
    return pltpu.make_async_remote_copy(
        src_ref=source,
        dst_ref=target,
        send_sem=send,
        recv_sem=recv,
        device_id=where,
        device_id_type=MESH,
    )


def dot(left, right):
    return jnp.dot(left, right, preferred_element_type=F32)


def column(row):
    count = row.shape[1]
    square = (count, count)
    same = lax.broadcasted_iota(jnp.int32, square, 0) == lax.broadcasted_iota(jnp.int32, square, 1)
    return jnp.sum(jnp.where(same, row, jnp.zeros_like(row)), axis=1, keepdims=True)


def layer_kernel(
    n_ep,
    n_tp,
    split,
    lengths_ref,
    lam_ref,
    resid_ref,
    first_gain_ref,
    head_gain_ref,
    gain_ref,
    mixw_ref,
    ids_ref,
    rw_ref,
    qw_hbm,
    kw_hbm,
    vw_hbm,
    cache_hbm,
    ow_hbm,
    eg_hbm,
    eu_hbm,
    ed_hbm,
    dg_hbm,
    du_hbm,
    dd_hbm,
    out_ref,
    new_ref,
    qw,
    kw,
    vw,
    cache,
    pairs,
    scores,
    mixed,
    heads_ref,
    ow,
    eg,
    eu,
    ed,
    dg,
    du,
    dd,
    heads_all,
    stream,
    ffn,
    mix,
    route,
    eh,
    dh,
    away,
    came,
    summed,
    landed,
    w_sem,
    q_sem,
    cache_sem,
    route_send,
    route_recv,
    heads_send,
    heads_recv,
    first_send,
    second_send,
    relay_send,
    stream_recv,
    pair_send,
    pair_recv,
    back_send,
    back_recv,
):
    e = lax.axis_index("ep")
    t = lax.axis_index("tp")
    half = n_tp // 2
    mate = flip(t, 1)
    core = t % 2
    seqs, width = resid_ref.shape
    quarter = out_ref.shape[1]
    held, _, part = eg.shape
    hid = dg.shape[1]
    rows_all = n_ep * seqs
    evens = [2 * i for i in range(1, half)]

    depth = qw.shape[0] // Q_CHUNKS
    q_loads = [
        pltpu.make_async_copy(
            qw_hbm.at[pl.ds(i * depth, depth), :], qw.at[pl.ds(i * depth, depth), :], q_sem.at[i]
        )
        for i in range(Q_CHUNKS)
    ] + [
        pltpu.make_async_copy(kw_hbm, kw, q_sem.at[Q_CHUNKS]),
        pltpu.make_async_copy(vw_hbm, vw, q_sem.at[Q_CHUNKS + 1]),
    ]
    for load in q_loads:
        load.start()
    cache_loads = [
        pltpu.make_async_copy(cache_hbm.at[s], cache.at[s], cache_sem.at[s]) for s in range(seqs)
    ]
    for load in cache_loads:
        load.start()

    barrier = pltpu.get_barrier_semaphore()

    def greet(index):
        where = (index // half, 2 * (index % half) + core)

        @pl.when(jnp.logical_or(where[0] != e, where[1] != t))
        def _():
            pl.semaphore_signal(barrier, inc=1, device_id=where, device_id_type=MESH)

    each(n_ep * half, greet)
    for i in range(half):
        pl.semaphore_signal(
            barrier, inc=1, device_id=(e, 2 * i + 1 - core), device_id_type=MESH
        )

    if split:
        cols = block(t, hid)
        dense_parts = (dg_hbm.at[:, cols], du_hbm.at[:, cols], dd_hbm.at[cols, :])
    else:
        dense_parts = (dg_hbm, du_hbm, dd_hbm)
    loads = [
        pltpu.make_async_copy(src, dst, w_sem.at[i])
        for i, (src, dst) in enumerate(
            zip((ow_hbm, eg_hbm, eu_hbm) + dense_parts[:2] + (ed_hbm, dense_parts[2]), (ow, eg, eu, dg, du, ed, dd))
        )
    ]

    lane = lax.broadcasted_iota(jnp.int32, (seqs, route.shape[1]), 1)
    table = jnp.zeros((seqs, route.shape[1]), F32)
    for k in range(ids_ref.shape[0]):
        wanted = column(ids_ref[k : k + 1, :])
        table = table + jnp.where(lane == wanted, column(rw_ref[k : k + 1, :]), 0.0)
    own_rows = block(e, seqs)
    route[own_rows, :] = table

    resid = resid_ref[...].astype(F32)
    mean_sq = jnp.mean(resid * resid, axis=-1, keepdims=True)
    normed = (resid * lax.rsqrt(mean_sq + EPS) * first_gain_ref[...]).astype(BF16)
    row = lax.broadcasted_iota(jnp.int32, (seqs, LANES), 0)
    entry = lax.broadcasted_iota(jnp.int32, (seqs, LANES), 1) % QK_DIM
    position = jnp.zeros((seqs, LANES), F32)
    for s in range(seqs):
        position = jnp.where(row == s, lengths_ref[s].astype(F32), position)
    turn = QK_DIM // 2
    power = (entry % turn).astype(F32) * (-1.0 / turn)
    angle = position * jnp.exp(power * math.log(10000.0))
    cosine = jnp.cos(angle)
    sine = jnp.where(entry < turn, -jnp.sin(angle), jnp.sin(angle))

    def rotate(values):
        other = jnp.where(
            entry < turn, pltpu.roll(values, LANES - turn, 1), pltpu.roll(values, turn, 1)
        )
        return (values * cosine + other * sine).astype(BF16).astype(F32)

    query = jnp.zeros((seqs, qw.shape[1]), F32)
    for i in range(Q_CHUNKS):
        q_loads[i].wait()
        query = query + dot(
            normed[:, i * depth : (i + 1) * depth], qw[i * depth : (i + 1) * depth, :]
        )
    for load in q_loads[Q_CHUNKS:]:
        load.wait()
    keys_raw = dot(normed, kw[...])
    values_raw = dot(normed, vw[...])
    for load in loads:
        load.start()

    groups, spots = cache.shape[1], cache.shape[2]
    share = query.shape[1] // LANES // groups
    lower = lax.broadcasted_iota(jnp.int32, (seqs, LANES), 1) < QK_DIM
    fresh = []
    for g in range(groups):
        key = rotate(keys_raw[:, g * LANES : (g + 1) * LANES])
        value = values_raw[:, g * LANES : (g + 1) * LANES].astype(BF16).astype(F32)
        new_ref[:, 2 * g * LANES : (2 * g + 1) * LANES] = key
        new_ref[:, (2 * g + 1) * LANES : (2 * g + 2) * LANES] = value
        fresh.append((key, value))
        for j in range(share):
            at = (g * share + j) * LANES
            head = rotate(query[:, at : at + LANES])
            pairs[g, :, j, :] = jnp.where(lower, head, 0.0)
            pairs[g, :, share + j, :] = jnp.where(lower, 0.0, head)

    pl.semaphore_wait(barrier, n_ep * half - 1 + half)

    def route_copy(d):
        there = (e + d) % n_ep
        return remote(
            route.at[own_rows, :],
            route.at[own_rows, :],
            route_send.at[d - 1],
            route_recv.at[d - 1],
            (there, t),
        )

    def route_wait(d):
        came_from = (e + n_ep - d) % n_ep
        spot = route.at[block(came_from, seqs), :]
        remote(spot, spot, route_send.at[d - 1], route_recv.at[d - 1], (e, t)).wait_recv()

    each(n_ep - 1, lambda i: route_copy(i + 1).start())

    scale = QK_DIM**-0.5
    lines = 2 * share
    for s in range(seqs):
        cache_loads[s].wait()
        for g in range(groups):
            both = pairs[g, s].astype(BF16)
            scores[g, s] = (
                lax.dot_general(
                    both,
                    cache[s, g, :, :LANES],
                    (((1,), (1,)), ((), ())),
                    preferred_element_type=F32,
                )
                * scale
            )
    length = jnp.zeros((seqs, lines, 1), jnp.int32)
    which = lax.broadcasted_iota(jnp.int32, (seqs, lines, 1), 0)
    for s in range(seqs):
        length = jnp.where(which == s, lengths_ref[s], length)
    place = lax.broadcasted_iota(jnp.int32, (seqs, lines, spots), 2)
    valid = place < length
    line = lax.broadcasted_iota(jnp.int32, (lines, 1), 0)
    for g in range(groups):
        key, value = fresh[g]
        latest = jnp.sum(pairs[g] * key[:, None, :], axis=-1, keepdims=True) * scale
        masked = jnp.where(valid, scores[g], -jnp.inf)
        top = jnp.maximum(jnp.max(masked, axis=-1, keepdims=True), latest)
        raised = jnp.exp(masked - top)
        raised_new = jnp.exp(latest - top)
        total = jnp.sum(raised, axis=-1, keepdims=True) + raised_new
        prob = raised / total
        prob_new = jnp.broadcast_to(raised_new / total, (seqs, lines, LANES))
        lam = jnp.zeros((lines, 1), F32)
        for j in range(share):
            lam = jnp.where(line == j, lam_ref[g * share + j], lam)
        scores[g] = prob - lam[None] * pltpu.roll(prob, share, 1)
        new_weight = (prob_new - lam[None] * pltpu.roll(prob_new, share, 1)).astype(BF16).astype(F32)
        fresh_part = new_weight * value[:, None, :]
        for s in range(seqs):
            mixed[g, s] = dot(scores[g, s].astype(BF16), cache[s, g, :, LANES:])
        whole = mixed[g] + fresh_part
        mean_sq = jnp.mean(whole * whole, axis=-1, keepdims=True)
        mixed[g] = whole * lax.rsqrt(mean_sq + EPS) * head_gain_ref[...][None]
        for j in range(share):
            at = (g * share + j) * LANES
            heads_ref[:, at : at + LANES] = mixed[g, :, j, :].astype(BF16)

    def heads_copy(mask):
        return remote(
            heads_ref,
            heads_all.at[mask - 1],
            heads_send.at[mask - 1],
            heads_recv.at[mask - 1],
            (e, flip(t, mask)),
        )

    for mask in range(n_tp - 1, 0, -1):
        heads_copy(mask).start()

    loads[0].wait()
    span = heads_ref.shape[1]
    total = dot(heads_ref[...], ow[block(t, span), :])
    for mask in range(1, n_tp):
        heads_copy(mask).wait_recv()
        total = total + dot(heads_all[mask - 1], ow[block(flip(t, mask), span), :])
    own_cols = block(t, quarter)
    own_stream = (resid_ref[:, own_cols].astype(F32) + total).astype(BF16)
    stream[own_rows, own_cols] = own_stream

    def spot(owner, column):
        return stream.at[block(owner, seqs), block(column, quarter)]

    def owner_of(d):
        return (e + n_ep - d) % n_ep

    def first(d):
        return remote(
            spot(e, t), spot(e, t), first_send.at[d], stream_recv.at[0, d], ((e + d) % n_ep, t)
        )

    def second(d, mask):
        index = mask // 2 if mask != 1 else 0
        where = spot(owner_of(d), t)
        return remote(
            where, where, second_send.at[index, d], stream_recv.at[mask, d], (e, flip(t, mask))
        )

    def relay(d, mask):
        where = spot(owner_of(d), flip(t, mask))
        return remote(
            where, where, relay_send.at[mask // 2 - 1, d], stream_recv.at[mask + 1, d], (e, mate)
        )

    def arrived(d, mask):
        where = spot(owner_of(d), flip(t, mask))
        remote(where, where, first_send.at[d], stream_recv.at[mask, d], (e, t)).wait_recv()

    def spread(d):
        for mask in evens:
            second(d, mask).start()
        second(d, 1).start()

    far_first = sorted(range(1, n_ep), key=lambda d: -min(d, n_ep - d)) if n_ep <= 16 else None
    near_first = [0] + far_first[::-1] if far_first is not None else None
    each(n_ep - 1 if far_first is None else 1, lambda i: first(i + 1).start(), order=None) if far_first is None else [
        first(d).start() for d in far_first
    ]

    def stage_two(d):
        if not (isinstance(d, int) and d == 0):
            arrived(d, 0)
        spread(d)

    def stage_three(d):
        for mask in evens:
            arrived(d, mask)
            relay(d, mask).start()

    def normalise(d):
        arrived(d, 1)
        for mask in evens:
            arrived(d, mask + 1)
        rows = block(owner_of(d), seqs)
        values = stream[rows, :].astype(F32)
        mean_sq = jnp.mean(values * values, axis=-1, keepdims=True)
        scaled = (values * lax.rsqrt(mean_sq + EPS) * gain_ref[...]).astype(BF16)
        ffn[rows, :] = scaled
        inner = jnp.sum(scaled.astype(F32) * mixw_ref[...], axis=-1, keepdims=True)
        mix[rows, :] = jnp.broadcast_to(jax.nn.sigmoid(inner), (seqs, LANES))

    if near_first is not None:
        for i, d in enumerate(near_first):
            stage_two(d)
            if i:
                stage_three(near_first[i - 1])
            if i > 1:
                normalise(near_first[i - 2])
        stage_three(near_first[-1])
        for d in near_first[-2:]:
            normalise(d)
    else:
        stage_two(0)
        each(n_ep - 1, lambda i: stage_two(i + 1))
        each(n_ep, stage_three)
        each(n_ep, normalise)
    each(n_ep - 1, lambda i: route_wait(i + 1))

    many = min(rows_all, 128)
    batches = rows_all // many
    for load in loads[1:5]:
        load.wait()

    def hidden(b):
        rows = block(b, many)
        a = ffn[rows, :]
        for j in range(held):
            eh[j, rows, :] = (jax.nn.silu(dot(a, eg[j])) * dot(a, eu[j])).astype(BF16)
        units = jax.nn.silu(dot(a, dg[...])) * dot(a, du[...])
        if not split:
            own = hid // n_tp
            unit = lax.broadcasted_iota(jnp.int32, units.shape, 1)
            units = jnp.where((unit >= t * own) & (unit < (t + 1) * own), units, 0.0)
        dh[rows, :] = units.astype(BF16)

    each(batches, hidden)
    for load in loads[5:]:
        load.wait()

    def result(b, q):
        rows = block(b, many)
        cols = block(q, quarter)
        total = mix[rows, :1] * dot(dh[rows, :], dd[:, cols])
        lanes = lax.broadcasted_iota(jnp.int32, (many, route.shape[1]), 1)
        for j in range(held):
            weight = jnp.sum(
                jnp.where(lanes == e * held + j, route[rows, :], 0.0), axis=1, keepdims=True
            )
            piece = dot(eh[j, rows, :], ed[j, :, cols]).astype(BF16)
            total = total + weight * piece.astype(F32)
        return total

    def pair(j):
        return remote(away.at[j], came.at[j], pair_send.at[j], pair_recv.at[j], (e, mate))

    for j in range(half):

        def leave(b, j=j):
            away[j, block(b, many), :] = result(b, 2 * j + 1 - core).astype(BF16)

        each(batches, leave)
        pair(j).start()

    me = e * half + t // 2

    def back(j, d):
        there = (e + d) % n_ep
        return remote(
            summed.at[j, block(there, seqs), :],
            landed.at[me],
            back_send.at[j, d],
            back_recv.at[me],
            (there, 2 * j + core),
        )

    def same(j, d):
        return jnp.logical_and(jnp.asarray(d == 0), 2 * j + core == t)

    for j in range(half):

        def keep(b, j=j):
            summed[j, block(b, many), :] = result(b, 2 * j + core).astype(BF16)

        each(batches, keep)
    for j in range(half):
        pair(j).wait_recv()

        def add(b, j=j):
            rows = block(b, many)
            summed[j, rows, :] = (summed[j, rows, :].astype(F32) + came[j, rows, :].astype(F32)).astype(BF16)

        each(batches, add)

        def send(d, j=j):
            @pl.when(jnp.logical_not(same(j, d)))
            def _():
                back(j, d).start()

        each(n_ep, send, order=None if far_first is None else far_first + [0])

    landed[me] = summed[t // 2, own_rows, :]

    def take(index):
        @pl.when(index != me)
        def _():
            where = landed.at[index]
            remote(where, where, back_send.at[0, 0], back_recv.at[index], (e, t)).wait_recv()

    each(n_ep * half, take)
    out_ref[...] = own_stream.astype(F32) + jnp.sum(landed[...].astype(F32), axis=0)

    for mask in range(1, n_tp):
        heads_copy(mask).wait_send()
    each(n_ep - 1, lambda i: route_copy(i + 1).wait_send())
    each(n_ep - 1, lambda i: first(i + 1).wait_send())

    def sent(d):
        second(d, 1).wait_send()
        for mask in evens:
            second(d, mask).wait_send()
            relay(d, mask).wait_send()

    each(n_ep, sent)
    for j in range(half):
        pair(j).wait_send()

        def gone(d, j=j):
            @pl.when(jnp.logical_not(same(j, d)))
            def _():
                back(j, d).wait_send()

        each(n_ep, gone)


def on_device(
    residual_in,
    lengths,
    kv_cache,
    norm_gain_attn,
    query_weight,
    key_weight,
    value_weight,
    diff_lambda,
    head_gain,
    out_weight,
    norm_gain_ffn,
    route_ids,
    route_weights,
    expert_gate,
    expert_up,
    expert_down,
    dense_gate,
    dense_up,
    dense_down,
    dense_mix,
):
    n_ep = lax.axis_size("ep")
    n_tp = lax.axis_size("tp")
    half = n_tp // 2
    seqs, width = residual_in.shape
    groups, spots = kv_cache.shape[1:3]
    share = diff_lambda.shape[0] // groups
    inner = query_weight.shape[1]
    quarter = out_weight.shape[1]
    held, _, part = expert_gate.shape
    rows = n_ep * seqs
    own = dense_gate.shape[1] // n_tp
    split = own % LANES == 0
    hid = own if split else dense_gate.shape[1]
    lanes = -(-n_ep * held // LANES) * LANES
    vmem = pl.BlockSpec(memory_space=pltpu.VMEM)
    smem = pl.BlockSpec(memory_space=pltpu.SMEM)
    hbm = pl.BlockSpec(memory_space=pl.ANY)
    dma = pltpu.SemaphoreType.DMA
    layer_out, fresh = pl.pallas_call(
        functools.partial(layer_kernel, n_ep, n_tp, split),
        out_shape=(
            jax.ShapeDtypeStruct((seqs, quarter), F32),
            jax.ShapeDtypeStruct((seqs, groups * kv_cache.shape[3]), F32),
        ),
        in_specs=[smem] * 2 + [vmem] * 7 + [hbm] * 11,
        out_specs=(vmem, vmem),
        scratch_shapes=[
            pltpu.VMEM(query_weight.shape, BF16),
            pltpu.VMEM(key_weight.shape, BF16),
            pltpu.VMEM(value_weight.shape, BF16),
            pltpu.VMEM(kv_cache.shape, BF16),
            pltpu.VMEM((groups, seqs, 2 * share, LANES), F32),
            pltpu.VMEM((groups, seqs, 2 * share, spots), F32),
            pltpu.VMEM((groups, seqs, 2 * share, LANES), F32),
            pltpu.VMEM((seqs, inner), BF16),
            pltpu.VMEM(out_weight.shape, BF16),
            pltpu.VMEM(expert_gate.shape, BF16),
            pltpu.VMEM(expert_up.shape, BF16),
            pltpu.VMEM(expert_down.shape, BF16),
            pltpu.VMEM((width, hid), BF16),
            pltpu.VMEM((width, hid), BF16),
            pltpu.VMEM((hid, width), BF16),
            pltpu.VMEM((n_tp - 1, seqs, inner), BF16),
            pltpu.VMEM((rows, width), BF16),
            pltpu.VMEM((rows, width), BF16),
            pltpu.VMEM((rows, LANES), F32),
            pltpu.VMEM((rows, lanes), F32),
            pltpu.VMEM((held, rows, part), BF16),
            pltpu.VMEM((rows, hid), BF16),
            pltpu.VMEM((half, rows, quarter), BF16),
            pltpu.VMEM((half, rows, quarter), BF16),
            pltpu.VMEM((half, rows, quarter), BF16),
            pltpu.VMEM((n_ep * half, seqs, quarter), BF16),
            dma((7,)),
            dma((Q_CHUNKS + 2,)),
            dma((seqs,)),
            dma((n_ep - 1,)),
            dma((n_ep - 1,)),
            dma((n_tp - 1,)),
            dma((n_tp - 1,)),
            dma((n_ep,)),
            dma((half, n_ep)),
            dma((max(half - 1, 1), n_ep)),
            dma((n_tp, n_ep)),
            dma((half,)),
            dma((half,)),
            dma((half, n_ep)),
            dma((n_ep * half,)),
        ],
        compiler_params=pltpu.CompilerParams(
            collective_id=0, has_side_effects=True, vmem_limit_bytes=60 * 1024 * 1024
        ),
    )(
        lengths,
        diff_lambda,
        residual_in,
        norm_gain_attn[None, :],
        head_gain[None, :],
        norm_gain_ffn[None, :],
        dense_mix[None, :],
        route_ids.T,
        route_weights.T,
        query_weight,
        key_weight,
        value_weight,
        kv_cache,
        out_weight,
        expert_gate,
        expert_up,
        expert_down,
        dense_gate,
        dense_up,
        dense_down,
    )
    new_rows = fresh.astype(BF16).reshape(seqs, groups, kv_cache.shape[3])
    return (layer_out.astype(BF16), new_rows)


def solution(mesh):
    placed = (
        P("ep", None),
        P("ep"),
        P("ep", "tp", None, None),
        P(),
        P(None, "tp"),
        P(None, "tp"),
        P(None, "tp"),
        P("tp"),
        P(),
        P(None, "tp"),
        P(),
        P("ep", None),
        P("ep", None),
        P("ep", None, "tp"),
        P("ep", None, "tp"),
        P("ep", "tp", None),
        P(None, "ep"),
        P(None, "ep"),
        P("ep", None),
        P(),
    )
    return jax.shard_map(
        on_device,
        mesh=mesh,
        in_specs=placed,
        out_specs=(P("ep", "tp"), P("ep", "tp", None)),
        check_vma=False,
    )
```

profile of v0, /device:TPU:0, one launch (start us, length us, event | category | flops | bytes accessed | tf_op | source)
XLA Modules:
  0.0 45.7 jit_solution(15091195352521071757)
XLA Ops:
  0.6 42.4 %shard_map.203 = (f32[16,512]{1,0:T(8,128)}, f32[16,256]{1,0:T(8,128)}) custom-call(s32[16]{0:T(128)} %lengths_ref.1, f32[4]{0:T(128)} %lam_ref.1, bf16[16,2048]{1,0:T(8,128)(2,1)} %resid_ref.1, f32[1,2048]{1,0:T(1,128)} %bitcast.8, f32[1,128]{1,0:T(1,128)} %bitcast.13, f32[1,2048]{1,0:T(1,128)} %bitcast.9, f32[1,2048]{1,0:T(1,128)} %bitcast.10, ...), custom_call_target="tpu_custom_call" | custom-call | tf_op jit(solution)/shard_map/pallas_call | solution.py:572
  43.0 1.4 %convert_element_type.6 = bf16[16,512]{1,0:T(8,128)(2,1)} convert(f32[16,512]{1,0:T(8,128)} %get-tuple-element.4) | non-fusion elementwise | flops 8192 | bytes 49152 | tf_op jit(solution)/shard_map/convert_element_type | solution.py:649
  44.4 1.3 %convert_bitcast_fusion = bf16[16,1,256]{2,0,1:T(8,128)(2,1)} fusion(f32[16,256]{1,0:T(8,128)} %get-tuple-element.5), kind=kLoop, calls=%fused_computation | loop fusion | flops 4096 | bytes 24576 | tf_op jit(solution)/shard_map/reshape | solution.py:648
where the time goes:
time: 46 us; the launch traced here: 45.7 us
  Pallas kernels  42.4 us (92%)
  other arithmetic  2.68 us (6%)
  between operations  0.65 us (1%)
    pallas_call x1, Pallas kernels, on_device(): pl.pallas_call(functools.partial(layer_kernel, n_ep, n_tp, split), out_sh...  42.4 us
    convert_element_type x1, other arithmetic, on_device(): return (layer_out.astype(BF16), new_rows)  1.37 us
    reshape x1, other arithmetic, on_device(): new_rows = fresh.astype(BF16).reshape(seqs, groups, kv_cache.shape[3])  1.32 us

commit v1 on v0

--- a/solution.py
+++ b/solution.py
@@ -15,6 +15,8 @@
 BF16 = jnp.bfloat16
 LANES = 128
 Q_CHUNKS = 4
+INNER = 2
+CORES = 2
 
 
 def flip(value, mask):
@@ -529,6 +531,713 @@
         each(n_ep, gone)
 
 
+def near_kernel(
+    n_ep,
+    n_tp,
+    lengths_hbm,
+    lam_hbm,
+    resid_hbm,
+    first_gain_hbm,
+    head_gain_hbm,
+    gain_hbm,
+    mixw_hbm,
+    ids_hbm,
+    rw_hbm,
+    qw_hbm,
+    kw_hbm,
+    vw_hbm,
+    cache_hbm,
+    ow_hbm,
+    eg_hbm,
+    eu_hbm,
+    ed_hbm,
+    dg_hbm,
+    du_hbm,
+    dd_hbm,
+    out_ref,
+    new_ref,
+    lengths_ref,
+    lam_ref,
+    resid_ref,
+    first_gain_ref,
+    head_gain_ref,
+    gain_ref,
+    mixw_ref,
+    ids_ref,
+    rw_ref,
+    qw,
+    kw,
+    vw,
+    cache,
+    pairs,
+    scores,
+    mixed,
+    heads_ref,
+    ow,
+    gu,
+    ed,
+    dg,
+    du,
+    dd,
+    heads_all,
+    mine,
+    stream,
+    ffn,
+    mix,
+    route,
+    eh,
+    dh,
+    leaving,
+    kept,
+    plane_in,
+    column_out,
+    column_in,
+    small_sem,
+    q_sem,
+    cache_sem,
+    w_sem,
+    e_sem,
+    push_send,
+    push_recv,
+    route_send,
+    route_recv,
+    heads_send,
+    heads_recv,
+    first_send,
+    second_send,
+    stream_recv,
+    plane_send,
+    plane_recv,
+    column_send,
+    column_recv,
+):
+    e = lax.axis_index("ep")
+    t = lax.axis_index("tp")
+    planes = n_ep // INNER
+    z = e // INNER
+    x = e % INNER
+    y = t // CORES
+    c = t % CORES
+    keeper = z % CORES
+    odd = (c + z) % CORES
+    turns = planes // CORES
+    seqs, width = resid_ref.shape
+    quarter = out_ref.shape[1]
+    part = eg_hbm.shape[2]
+    hid = dg.shape[1]
+    mate = flip(t, 1)
+
+    small_loads = [
+        pltpu.make_async_copy(src, dst, small_sem.at[i])
+        for i, (src, dst) in enumerate(
+            (
+                (resid_hbm, resid_ref),
+                (first_gain_hbm, first_gain_ref),
+                (lengths_hbm, lengths_ref),
+                (ids_hbm, ids_ref),
+                (rw_hbm, rw_ref),
+                (lam_hbm, lam_ref),
+                (head_gain_hbm, head_gain_ref),
+                (gain_hbm, gain_ref),
+                (mixw_hbm, mixw_ref),
+            )
+        )
+    ]
+    for load in small_loads:
+        load.start()
+    depth = qw.shape[0] // Q_CHUNKS
+    q_loads = [
+        pltpu.make_async_copy(
+            qw_hbm.at[pl.ds(i * depth, depth), :], qw.at[pl.ds(i * depth, depth), :], q_sem.at[i]
+        )
+        for i in range(Q_CHUNKS)
+    ] + [
+        pltpu.make_async_copy(kw_hbm, kw, q_sem.at[Q_CHUNKS]),
+        pltpu.make_async_copy(vw_hbm, vw, q_sem.at[Q_CHUNKS + 1]),
+    ]
+    for load in q_loads:
+        load.start()
+    e_loads = [
+        pltpu.make_async_copy(eg_hbm.at[0], gu.at[c, :, :part], e_sem.at[0]),
+        pltpu.make_async_copy(eu_hbm.at[0], gu.at[c, :, part:], e_sem.at[1]),
+        pltpu.make_async_copy(ed_hbm.at[0], ed.at[block(c, part), :], e_sem.at[2]),
+    ]
+    for load in e_loads:
+        load.start()
+    cache_loads = [
+        pltpu.make_async_copy(cache_hbm.at[s], cache.at[s], cache_sem.at[s]) for s in range(seqs)
+    ]
+    for load in cache_loads:
+        load.start()
+
+    barrier = pltpu.get_barrier_semaphore()
+    for index in range(n_ep * n_tp):
+        where = (index // n_tp, index % n_tp)
+
+        @pl.when(jnp.logical_or(where[0] != e, where[1] != t))
+        def _():
+            pl.semaphore_signal(barrier, inc=1, device_id=where, device_id_type=MESH)
+
+    cols = block(y, hid)
+    loads = [
+        pltpu.make_async_copy(src, dst, w_sem.at[i])
+        for i, (src, dst) in enumerate(
+            (
+                (ow_hbm, ow),
+                (dg_hbm.at[:, cols], dg),
+                (du_hbm.at[:, cols], du),
+                (dd_hbm.at[cols, :], dd),
+            )
+        )
+    ]
+
+    for load in small_loads[:3]:
+        load.wait()
+    resid = resid_ref[...].astype(F32)
+    mean_sq = jnp.mean(resid * resid, axis=-1, keepdims=True)
+    normed = (resid * lax.rsqrt(mean_sq + EPS) * first_gain_ref[...]).astype(BF16)
+    row = lax.broadcasted_iota(jnp.int32, (seqs, LANES), 0)
+    entry = lax.broadcasted_iota(jnp.int32, (seqs, LANES), 1) % QK_DIM
+    position = jnp.zeros((seqs, LANES), F32)
+    for s in range(seqs):
+        position = jnp.where(row == s, lengths_ref[s].astype(F32), position)
+    turn = QK_DIM // 2
+    power = (entry % turn).astype(F32) * (-1.0 / turn)
+    angle = position * jnp.exp(power * math.log(10000.0))
+    cosine = jnp.cos(angle)
+    sine = jnp.where(entry < turn, -jnp.sin(angle), jnp.sin(angle))
+
+    def rotate(values):
+        other = jnp.where(
+            entry < turn, pltpu.roll(values, LANES - turn, 1), pltpu.roll(values, turn, 1)
+        )
+        return (values * cosine + other * sine).astype(BF16).astype(F32)
+
+    for load in small_loads[3:]:
+        load.wait()
+
+    def spot(plane, inner):
+        return plane // CORES * INNER + inner
+
+    own_spot = spot(z, x)
+    lane = lax.broadcasted_iota(jnp.int32, (seqs, route.shape[2]), 1)
+    table = jnp.zeros((seqs, route.shape[2]), F32)
+    for k in range(ids_ref.shape[0]):
+        wanted = column(ids_ref[k : k + 1, :])
+        table = table + jnp.where(lane == wanted, column(rw_ref[k : k + 1, :]), 0.0)
+
+    @pl.when(odd == 0)
+    def _():
+        route[own_spot] = table
+
+    query = jnp.zeros((seqs, qw.shape[1]), F32)
+    for i in range(Q_CHUNKS):
+        q_loads[i].wait()
+        query = query + dot(
+            normed[:, i * depth : (i + 1) * depth], qw[i * depth : (i + 1) * depth, :]
+        )
+    for load in q_loads[Q_CHUNKS:]:
+        load.wait()
+    keys_raw = dot(normed, kw[...])
+    values_raw = dot(normed, vw[...])
+    for load in loads:
+        load.start()
+
+    groups, spots = cache.shape[1], cache.shape[2]
+    share = query.shape[1] // LANES // groups
+    lower = lax.broadcasted_iota(jnp.int32, (seqs, LANES), 1) < QK_DIM
+    fresh = []
+    for g in range(groups):
+        key = rotate(keys_raw[:, g * LANES : (g + 1) * LANES])
+        value = values_raw[:, g * LANES : (g + 1) * LANES].astype(BF16).astype(F32)
+        new_ref[:, 2 * g * LANES : (2 * g + 1) * LANES] = key.astype(BF16)
+        new_ref[:, (2 * g + 1) * LANES : (2 * g + 2) * LANES] = value.astype(BF16)
+        fresh.append((key, value))
+        for j in range(share):
+            at = (g * share + j) * LANES
+            head = rotate(query[:, at : at + LANES])
+            pairs[g, :, j, :] = jnp.where(lower, head, 0.0)
+            pairs[g, :, share + j, :] = jnp.where(lower, 0.0, head)
+
+    pl.semaphore_wait(barrier, n_ep * n_tp - 1)
+
+    def push(index):
+        where = (gu.at[c], ed.at[block(c, part), :])[index]
+        return remote(where, where, push_send.at[index], push_recv.at[index], (e, mate))
+
+    def pushed(index):
+        where = (gu.at[1 - c], ed.at[block(1 - c, part), :])[index]
+        remote(where, where, push_send.at[index], push_recv.at[index], (e, mate)).wait_recv()
+
+    for load in e_loads:
+        load.wait()
+    push(0).start()
+    push(1).start()
+
+    def route_copy(mask):
+        where = route.at[own_spot]
+        return remote(
+            where, where, route_send.at[mask - 1], route_recv.at[own_spot], (flip(e, mask), t)
+        )
+
+    @pl.when(odd == 0)
+    def _():
+        for mask in range(1, n_ep):
+            route_copy(mask).start()
+
+    scale = QK_DIM**-0.5
+    lines = 2 * share
+    for s in range(seqs):
+        cache_loads[s].wait()
+        for g in range(groups):
+            both = pairs[g, s].astype(BF16)
+            scores[g, s] = (
+                lax.dot_general(
+                    both,
+                    cache[s, g, :, :LANES],
+                    (((1,), (1,)), ((), ())),
+                    preferred_element_type=F32,
+                )
+                * scale
+            )
+    length = jnp.zeros((seqs, lines, 1), jnp.int32)
+    which = lax.broadcasted_iota(jnp.int32, (seqs, lines, 1), 0)
+    for s in range(seqs):
+        length = jnp.where(which == s, lengths_ref[s], length)
+    place = lax.broadcasted_iota(jnp.int32, (seqs, lines, spots), 2)
+    valid = place < length
+    line = lax.broadcasted_iota(jnp.int32, (lines, 1), 0)
+    for g in range(groups):
+        key, value = fresh[g]
+        latest = jnp.sum(pairs[g] * key[:, None, :], axis=-1, keepdims=True) * scale
+        masked = jnp.where(valid, scores[g], -jnp.inf)
+        top = jnp.maximum(jnp.max(masked, axis=-1, keepdims=True), latest)
+        raised = jnp.exp(masked - top)
+        raised_new = jnp.exp(latest - top)
+        total = jnp.sum(raised, axis=-1, keepdims=True) + raised_new
+        prob = raised / total
+        prob_new = jnp.broadcast_to(raised_new / total, (seqs, lines, LANES))
+        lam = jnp.zeros((lines, 1), F32)
+        for j in range(share):
+            lam = jnp.where(line == j, lam_ref[g * share + j], lam)
+        scores[g] = prob - lam[None] * pltpu.roll(prob, share, 1)
+        new_weight = (prob_new - lam[None] * pltpu.roll(prob_new, share, 1)).astype(BF16).astype(F32)
+        fresh_part = new_weight * value[:, None, :]
+        for s in range(seqs):
+            mixed[g, s] = dot(scores[g, s].astype(BF16), cache[s, g, :, LANES:])
+        whole = mixed[g] + fresh_part
+        mean_sq = jnp.mean(whole * whole, axis=-1, keepdims=True)
+        mixed[g] = whole * lax.rsqrt(mean_sq + EPS) * head_gain_ref[...][None]
+        for j in range(share):
+            at = (g * share + j) * LANES
+            heads_ref[:, at : at + LANES] = mixed[g, :, j, :].astype(BF16)
+
+    def heads_copy(mask):
+        return remote(
+            heads_ref,
+            heads_all.at[mask - 1],
+            heads_send.at[mask - 1],
+            heads_recv.at[mask - 1],
+            (e, flip(t, mask)),
+        )
+
+    for mask in range(n_tp - 1, 0, -1):
+        heads_copy(mask).start()
+
+    loads[0].wait()
+    span = heads_ref.shape[1]
+    total = dot(heads_ref[...], ow[block(t, span), :])
+    for mask in range(1, n_tp):
+        heads_copy(mask).wait_recv()
+        total = total + dot(heads_all[mask - 1], ow[block(flip(t, mask), span), :])
+    own_cols = block(t, quarter)
+    own_stream = (resid_ref[:, own_cols].astype(F32) + total).astype(BF16)
+    mine[...] = own_stream
+
+    around = ((1, 1), (1, 0), (0, 1))
+
+    def at_spot(where, owner):
+        return stream.at[block(where, seqs), block(owner, quarter)]
+
+    def to_plane(step):
+        dx, dy = around[step]
+        there = (z * INNER + flip(x, dx), flip(y, dy) * CORES + keeper)
+        return remote(
+            mine, at_spot(own_spot, t), first_send.at[step], stream_recv.at[own_spot, t], there
+        )
+
+    def to_column(d):
+        there = (flip(z, d) * INNER + x, y * CORES + keeper)
+        return remote(
+            mine,
+            at_spot(own_spot, t),
+            first_send.at[len(around) + d],
+            stream_recv.at[own_spot, t],
+            there,
+        )
+
+    def to_mate():
+        return remote(
+            mine,
+            at_spot(own_spot, t),
+            first_send.at[len(around)],
+            stream_recv.at[own_spot, t],
+            (e, mate),
+        )
+
+    for d in range(planes - 1, 0, -1):
+        to_column(d).start()
+    for step in range(len(around)):
+        to_plane(step).start()
+
+    @pl.when(odd == 1)
+    def _():
+        to_mate().start()
+
+    @pl.when(odd == 0)
+    def _():
+        stream[block(own_spot, seqs), own_cols] = own_stream
+
+    near = z + odd * (1 - 2 * (z % 2))
+
+    def plane_of(i):
+        return flip(near, 2 * i)
+
+    def arrived(where, owner):
+        spot_ref = at_spot(where, owner)
+        remote(
+            spot_ref, spot_ref, first_send.at[0], stream_recv.at[where, owner], (e, t)
+        ).wait_recv()
+
+    def forward(i, core, step):
+        dx, dy = around[step]
+        owner = y * CORES + core
+        where = spot(plane_of(i), x)
+        spot_ref = at_spot(where, owner)
+        return remote(
+            spot_ref,
+            spot_ref,
+            second_send.at[i, core, step],
+            stream_recv.at[where, owner],
+            (z * INNER + flip(x, dx), flip(y, dy) * CORES + c),
+        )
+
+    def relay(i):
+        for core in range(CORES):
+            arrived(spot(plane_of(i), x), y * CORES + core)
+            for step in range(len(around)):
+                forward(i, core, step).start()
+
+    def gather(i):
+        if i == 0:
+
+            @pl.when(odd == 1)
+            def _():
+                relay(0)
+
+            @pl.when(odd == 0)
+            def _():
+                arrived(own_spot, mate)
+        else:
+            relay(i)
+
+    def normalise(i):
+        for inner in (0, 1):
+            where = spot(plane_of(i), flip(x, inner))
+            for core in range(CORES):
+                arrived(where, flip(y, 1) * CORES + core)
+            if inner:
+                for core in range(CORES):
+                    arrived(where, y * CORES + core)
+            rows = block(where, seqs)
+            values = stream[rows, :].astype(F32)
+            mean_sq = jnp.mean(values * values, axis=-1, keepdims=True)
+            scaled = (values * lax.rsqrt(mean_sq + EPS) * gain_ref[...]).astype(BF16)
+            ffn[rows, :] = scaled
+            inside = jnp.sum(scaled.astype(F32) * mixw_ref[...], axis=-1, keepdims=True)
+            mix[rows, :] = jnp.broadcast_to(jax.nn.sigmoid(inside), (seqs, LANES))
+
+    for i in range(turns):
+        gather(i)
+    for i in range(turns):
+        normalise(i)
+
+    for i in range(turns):
+        for inner in range(INNER):
+            where = spot(plane_of(i), inner)
+
+            def route_wait(where=where):
+                spot_ref = route.at[where]
+                remote(
+                    spot_ref, spot_ref, route_send.at[0], route_recv.at[where], (e, t)
+                ).wait_recv()
+
+            if i == 0:
+
+                @pl.when(jnp.logical_or(odd == 1, inner != x))
+                def _():
+                    route_wait()
+            else:
+                route_wait()
+
+    rows_all = ffn.shape[0]
+    pushed(0)
+    pushed(1)
+    for load in loads[1:3]:
+        load.wait()
+    a = ffn[...]
+    for core in range(CORES):
+        both = dot(a, gu[core])
+        eh[:, core * part : (core + 1) * part] = (
+            jax.nn.silu(both[:, :part]) * both[:, part:]
+        ).astype(BF16)
+    dh[...] = (jax.nn.silu(dot(a, dg[...])) * dot(a, du[...])).astype(BF16)
+    loads[3].wait()
+
+    lanes = lax.broadcasted_iota(jnp.int32, (rows_all, route.shape[2]), 1)
+    weight = jnp.sum(
+        jnp.where(lanes == e, route[...].reshape(rows_all, route.shape[2]), 0.0),
+        axis=1,
+        keepdims=True,
+    )
+
+    def leave(i, dy, core, step):
+        dx = around[step][0]
+        where = spot(plane_of(i), flip(x, dx))
+        return remote(
+            leaving.at[dy, core, block(where, seqs), :],
+            plane_in.at[i, core, step],
+            plane_send.at[i, core, step],
+            plane_recv.at[i, core, step],
+            (z * INNER + flip(x, dx), flip(y, dy) * CORES + c),
+        )
+
+    order = range(turns - 1, -1, -1)
+    for dy in (1, 0):
+        for core in range(CORES):
+            cols = block(flip(y, dy) * CORES + core, quarter)
+            total = mix[:, :1] * dot(dh[...], dd[:, cols]) + weight * dot(eh[...], ed[:, cols])
+            leaving[dy, core] = total.astype(BF16)
+            if not dy:
+                kept[core] = total
+            for i in order:
+                for step in range(len(around)):
+                    if around[step][1] == dy:
+                        leave(i, dy, core, step).start()
+
+    def own_plane(i):
+        return jnp.logical_and(odd == 0, i == 0)
+
+    def climb(i, core):
+        return remote(
+            column_out.at[i, core],
+            column_in.at[odd + 2 * i],
+            column_send.at[i, core],
+            column_recv.at[odd + 2 * i],
+            (plane_of(i) * INNER + x, y * CORES + core),
+        )
+
+    def stays(i, core):
+        return jnp.logical_and(own_plane(i), c == core)
+
+    for i in order:
+        for core in range(CORES):
+            gathered = kept[core, block(spot(plane_of(i), x), seqs), :]
+            for step in range(len(around)):
+                leave(i, around[step][1], core, step).wait_recv()
+                gathered = gathered + plane_in[i, core, step].astype(F32)
+            column_out[i, core] = gathered.astype(BF16)
+
+            @pl.when(jnp.logical_not(stays(i, core)))
+            def _(i=i, core=core):
+                climb(i, core).start()
+
+    def took(d):
+        where = column_in.at[d]
+        remote(where, where, column_send.at[0, 0], column_recv.at[d], (e, t)).wait_recv()
+
+    @pl.when(odd == 0)
+    def _():
+        column_in[0] = column_out[0, c]
+
+    @pl.when(odd == 1)
+    def _():
+        took(0)
+
+    for d in range(1, planes):
+        took(d)
+    out_ref[...] = (
+        own_stream.astype(F32) + jnp.sum(column_in[...].astype(F32), axis=0)
+    ).astype(BF16)
+
+    push(0).wait_send()
+    push(1).wait_send()
+    for mask in range(1, n_tp):
+        heads_copy(mask).wait_send()
+
+    @pl.when(odd == 0)
+    def _():
+        for mask in range(1, n_ep):
+            route_copy(mask).wait_send()
+
+    for d in range(1, planes):
+        to_column(d).wait_send()
+    for step in range(len(around)):
+        to_plane(step).wait_send()
+
+    @pl.when(odd == 1)
+    def _():
+        to_mate().wait_send()
+
+    for i in range(turns):
+        for core in range(CORES):
+            for step in range(len(around)):
+
+                def forwarded(i=i, core=core, step=step):
+                    forward(i, core, step).wait_send()
+
+                if i == 0:
+                    pl.when(odd == 1)(forwarded)
+                else:
+                    forwarded()
+                leave(i, around[step][1], core, step).wait_send()
+
+            @pl.when(jnp.logical_not(stays(i, core)))
+            def _(i=i, core=core):
+                climb(i, core).wait_send()
+
+
+def near_call(n_ep, n_tp, arrays):
+    (
+        residual_in,
+        lengths,
+        kv_cache,
+        norm_gain_attn,
+        query_weight,
+        key_weight,
+        value_weight,
+        diff_lambda,
+        head_gain,
+        out_weight,
+        norm_gain_ffn,
+        route_ids,
+        route_weights,
+        expert_gate,
+        expert_up,
+        expert_down,
+        dense_gate,
+        dense_up,
+        dense_down,
+        dense_mix,
+    ) = arrays
+    seqs, width = residual_in.shape
+    held = lambda value: pltpu.with_memory_space_constraint(value, pltpu.HBM)
+    groups, spots = kv_cache.shape[1:3]
+    share = diff_lambda.shape[0] // groups
+    inner = query_weight.shape[1]
+    quarter = out_weight.shape[1]
+    part = expert_gate.shape[2]
+    hid = dense_gate.shape[1] // (n_tp // CORES)
+    turns = n_ep // INNER // CORES
+    blocks = turns * INNER
+    rows = blocks * seqs
+    lanes = -(-n_ep // LANES) * LANES
+    topk = route_ids.shape[1]
+    vmem = pl.BlockSpec(memory_space=pltpu.VMEM)
+    hbm = pl.BlockSpec(memory_space=pltpu.HBM)
+    dma = pltpu.SemaphoreType.DMA
+    layer_out, fresh = pl.pallas_call(
+        functools.partial(near_kernel, n_ep, n_tp),
+        out_shape=(
+            jax.ShapeDtypeStruct((seqs, quarter), BF16),
+            jax.ShapeDtypeStruct((seqs, groups * kv_cache.shape[3]), BF16),
+        ),
+        in_specs=[hbm] * 20,
+        out_specs=(vmem, vmem),
+        scratch_shapes=[
+            pltpu.SMEM(lengths.shape, jnp.int32),
+            pltpu.SMEM(diff_lambda.shape, F32),
+            pltpu.VMEM(residual_in.shape, BF16),
+            pltpu.VMEM((1, width), F32),
+            pltpu.VMEM((1, head_gain.shape[0]), F32),
+            pltpu.VMEM((1, width), F32),
+            pltpu.VMEM((1, width), F32),
+            pltpu.VMEM((topk, seqs), jnp.int32),
+            pltpu.VMEM((topk, seqs), F32),
+            pltpu.VMEM(query_weight.shape, BF16),
+            pltpu.VMEM(key_weight.shape, BF16),
+            pltpu.VMEM(value_weight.shape, BF16),
+            pltpu.VMEM(kv_cache.shape, BF16),
+            pltpu.VMEM((groups, seqs, 2 * share, LANES), F32),
+            pltpu.VMEM((groups, seqs, 2 * share, spots), F32),
+            pltpu.VMEM((groups, seqs, 2 * share, LANES), F32),
+            pltpu.VMEM((seqs, inner), BF16),
+            pltpu.VMEM(out_weight.shape, BF16),
+            pltpu.VMEM((CORES, width, 2 * part), BF16),
+            pltpu.VMEM((CORES * part, width), BF16),
+            pltpu.VMEM((width, hid), BF16),
+            pltpu.VMEM((width, hid), BF16),
+            pltpu.VMEM((hid, width), BF16),
+            pltpu.VMEM((n_tp - 1, seqs, inner), BF16),
+            pltpu.VMEM((seqs, quarter), BF16),
+            pltpu.VMEM((rows, width), BF16),
+            pltpu.VMEM((rows, width), BF16),
+            pltpu.VMEM((rows, LANES), F32),
+            pltpu.VMEM((blocks, seqs, lanes), F32),
+            pltpu.VMEM((rows, CORES * part), BF16),
+            pltpu.VMEM((rows, hid), BF16),
+            pltpu.VMEM((2, CORES, rows, quarter), BF16),
+            pltpu.VMEM((CORES, rows, quarter), F32),
+            pltpu.VMEM((turns, CORES, 3, seqs, quarter), BF16),
+            pltpu.VMEM((turns, CORES, seqs, quarter), BF16),
+            pltpu.VMEM((n_ep // INNER, seqs, quarter), BF16),
+            dma((9,)),
+            dma((Q_CHUNKS + 2,)),
+            dma((seqs,)),
+            dma((4,)),
+            dma((3,)),
+            dma((2,)),
+            dma((2,)),
+            dma((n_ep - 1,)),
+            dma((blocks,)),
+            dma((n_tp - 1,)),
+            dma((n_tp - 1,)),
+            dma((3 + n_ep // INNER,)),
+            dma((turns, CORES, 3)),
+            dma((blocks, n_tp)),
+            dma((turns, CORES, 3)),
+            dma((turns, CORES, 3)),
+            dma((turns, CORES)),
+            dma((n_ep // INNER,)),
+        ],
+        compiler_params=pltpu.CompilerParams(
+            collective_id=0, has_side_effects=True, vmem_limit_bytes=36 * 1024 * 1024
+        ),
+    )(
+        held(lengths),
+        held(diff_lambda),
+        held(residual_in),
+        held(norm_gain_attn[None, :]),
+        held(head_gain[None, :]),
+        held(norm_gain_ffn[None, :]),
+        held(dense_mix[None, :]),
+        held(route_ids.T),
+        held(route_weights.T),
+        held(query_weight),
+        held(key_weight),
+        held(value_weight),
+        held(kv_cache),
+        held(out_weight),
+        held(expert_gate),
+        held(expert_up),
+        held(expert_down),
+        held(dense_gate),
+        held(dense_up),
+        held(dense_down),
+    )
+    return layer_out, fresh.reshape(seqs, groups, kv_cache.shape[3])
+
+
 def on_device(
     residual_in,
     lengths,
@@ -554,6 +1263,39 @@
     n_ep = lax.axis_size("ep")
     n_tp = lax.axis_size("tp")
     half = n_tp // 2
+    if (
+        n_tp == 2 * CORES
+        and n_ep in (4, 8, 16)
+        and expert_gate.shape[0] == 1
+        and dense_gate.shape[1] // half % LANES == 0
+        and expert_gate.shape[2] % LANES == 0
+    ):
+        return near_call(
+            n_ep,
+            n_tp,
+            (
+                residual_in,
+                lengths,
+                kv_cache,
+                norm_gain_attn,
+                query_weight,
+                key_weight,
+                value_weight,
+                diff_lambda,
+                head_gain,
+                out_weight,
+                norm_gain_ffn,
+                route_ids,
+                route_weights,
+                expert_gate,
+                expert_up,
+                expert_down,
+                dense_gate,
+                dense_up,
+                dense_down,
+                dense_mix,
+            ),
+        )
     seqs, width = residual_in.shape
     groups, spots = kv_cache.shape[1:3]
     share = diff_lambda.shape[0] // groups

time: 46 us -> 33.3 us (0.72)
  Pallas kernels: 42.4 us -> 31.3 us
  other arithmetic: 2.68 us -> 0 us
  local copies, waits for them, and re-layouts: 0 us -> 1.21 us
    pallas_call x1, Pallas kernels: 42.4 us -> 31.3 us  [near_call(): pl.pallas_call(functools.partial(near_kernel, n_ep, n_tp), out_shape=(jax...]
    convert_element_type x1 -> x0, other arithmetic: 1.37 us -> none  [on_device(): return (layer_out.astype(BF16), new_rows)]
    reshape x1 -> x0, other arithmetic: 1.32 us -> none  [on_device(): new_rows = fresh.astype(BF16).reshape(seqs, groups, kv_cache.shape[3])]
    unnamed x0 -> x2, local copies, waits for them, and re-layouts: none -> 1.21 us
where the time goes in v1:
time: 33.3 us; the launch traced here: 33.1 us
  Pallas kernels  31.3 us (94%)
  local copies, waits for them, and re-layouts  1.21 us (4%)
  between operations  0.65 us (2%)
    pallas_call x1, Pallas kernels, near_call(): pl.pallas_call(functools.partial(near_kernel, n_ep, n_tp), out_shape=(jax...  31.3 us
    unnamed x2, local copies, waits for them, and re-layouts  1.21 us

profile of v1, /device:TPU:0, one launch (start us, length us, event | category | flops | bytes accessed | tf_op | source)
XLA Modules:
  0.0 33.1 jit_solution(14623446201535716932)
XLA Ops:
  0.6 31.3 %shard_map.203 = (bf16[16,512]{1,0:T(8,128)(2,1)S(1)}, bf16[16,256]{1,0:T(8,128)(2,1)S(1)}) custom-call(s32[16]{0:T(128)} %lengths_hbm.1, f32[4]{0:T(128)} %lam_hbm.1, bf16[16,2048]{1,0:T(8,128)(2,1)} %resid_hbm.1, f32[1,2048]{1,0:T(1,128)} %bitcast.8, f32[1,128]{1,0:T(1,128)} %bitcast.13, f32[1,2048]{1,0:T(1,128)} %bitcast.9, f32[1,2048]{1,0:T(1,128)} %bitcast.10, ...), custom_call_target="tpu_custom_call" | custom-call | tf_op jit(solution)/shard_map/pallas_call | solution.py:1149
  31.9 0.6 %copy.24 = bf16[16,512]{1,0:T(8,128)(2,1)} copy(bf16[16,512]{1,0:T(8,128)(2,1)S(1)} %get-tuple-element.8) | data formatting | bytes 32768
  32.5 0.6 %copy.25 = bf16[16,1,256]{2,0,1:T(8,128)(2,1)} copy(bf16[16,1,256]{2,0,1:T(8,128)(2,1)S(1)} %bitcast.7) | data formatting | bytes 16384

commit v2 on v1

--- a/solution.py
+++ b/solution.py
@@ -17,6 +17,7 @@
 Q_CHUNKS = 4
 INNER = 2
 CORES = 2
+CACHE_CHUNKS = 4
 
 
 def flip(value, mask):
@@ -565,11 +566,10 @@
     mixw_ref,
     ids_ref,
     rw_ref,
-    qw,
-    kw,
-    vw,
+    qkv,
     cache,
     pairs,
+    asked,
     scores,
     mixed,
     heads_ref,
@@ -592,23 +592,17 @@
     plane_in,
     column_out,
     column_in,
-    small_sem,
-    q_sem,
-    cache_sem,
-    w_sem,
-    e_sem,
+    local_sem,
     push_send,
     push_recv,
     route_send,
     route_recv,
     heads_send,
     heads_recv,
-    first_send,
-    second_send,
-    stream_recv,
-    plane_send,
+    chunk_send,
+    climb_recv,
+    group_recv,
     plane_recv,
-    column_send,
     column_recv,
 ):
     e = lax.axis_index("ep")
@@ -627,61 +621,66 @@
     hid = dg.shape[1]
     mate = flip(t, 1)
 
-    small_loads = [
-        pltpu.make_async_copy(src, dst, small_sem.at[i])
-        for i, (src, dst) in enumerate(
-            (
-                (resid_hbm, resid_ref),
-                (first_gain_hbm, first_gain_ref),
-                (lengths_hbm, lengths_ref),
-                (ids_hbm, ids_ref),
-                (rw_hbm, rw_ref),
-                (lam_hbm, lam_ref),
-                (head_gain_hbm, head_gain_ref),
-                (gain_hbm, gain_ref),
-                (mixw_hbm, mixw_ref),
-            )
-        )
-    ]
-    for load in small_loads:
+    def gather_loads(sem, *routes):
+        return [pltpu.make_async_copy(src, dst, local_sem.at[sem]) for src, dst in routes]
+
+    first_loads = gather_loads(
+        0, (resid_hbm, resid_ref), (first_gain_hbm, first_gain_ref), (lengths_hbm, lengths_ref)
+    )
+    for load in first_loads:
         load.start()
-    depth = qw.shape[0] // Q_CHUNKS
-    q_loads = [
-        pltpu.make_async_copy(
-            qw_hbm.at[pl.ds(i * depth, depth), :], qw.at[pl.ds(i * depth, depth), :], q_sem.at[i]
-        )
-        for i in range(Q_CHUNKS)
-    ] + [
-        pltpu.make_async_copy(kw_hbm, kw, q_sem.at[Q_CHUNKS]),
-        pltpu.make_async_copy(vw_hbm, vw, q_sem.at[Q_CHUNKS + 1]),
-    ]
-    for load in q_loads:
-        load.start()
-    e_loads = [
-        pltpu.make_async_copy(eg_hbm.at[0], gu.at[c, :, :part], e_sem.at[0]),
-        pltpu.make_async_copy(eu_hbm.at[0], gu.at[c, :, part:], e_sem.at[1]),
-        pltpu.make_async_copy(ed_hbm.at[0], ed.at[block(c, part), :], e_sem.at[2]),
-    ]
-    for load in e_loads:
-        load.start()
+    depth = qkv.shape[0] // Q_CHUNKS
+    inner = qw_hbm.shape[1]
+    side = kw_hbm.shape[1]
+    for i in range(Q_CHUNKS):
+        deep = pl.ds(i * depth, depth)
+        for load in gather_loads(
+            1 + i,
+            (qw_hbm.at[deep, :], qkv.at[deep, :inner]),
+            (kw_hbm.at[deep, :], qkv.at[deep, inner : inner + side]),
+            (vw_hbm.at[deep, :], qkv.at[deep, inner + side :]),
+        ):
+            load.start()
+
+    barrier = pltpu.get_barrier_semaphore()
+    for index in range(n_ep * n_tp):
+        where = (index // n_tp, index % n_tp)
+
+        @pl.when(jnp.logical_or(where[0] != e, where[1] != t))
+        def _():
+            pl.semaphore_signal(barrier, inc=1, device_id=where, device_id_type=MESH)
+
+    for load in first_loads:
+        load.wait()
+    bunch = seqs // CACHE_CHUNKS
     cache_loads = [
-        pltpu.make_async_copy(cache_hbm.at[s], cache.at[s], cache_sem.at[s]) for s in range(seqs)
+        gather_loads(
+            1 + Q_CHUNKS + i,
+            (cache_hbm.at[pl.ds(i * bunch, bunch)], cache.at[pl.ds(i * bunch, bunch)]),
+        )[0]
+        for i in range(CACHE_CHUNKS)
     ]
     for load in cache_loads:
         load.start()
-
-    barrier = pltpu.get_barrier_semaphore()
-    for index in range(n_ep * n_tp):
-        where = (index // n_tp, index % n_tp)
-
-        @pl.when(jnp.logical_or(where[0] != e, where[1] != t))
-        def _():
-            pl.semaphore_signal(barrier, inc=1, device_id=where, device_id_type=MESH)
-
+    late = 1 + Q_CHUNKS + CACHE_CHUNKS
+    late_loads = gather_loads(
+        late,
+        (ids_hbm, ids_ref),
+        (rw_hbm, rw_ref),
+        (lam_hbm, lam_ref),
+        (head_gain_hbm, head_gain_ref),
+        (gain_hbm, gain_ref),
+        (mixw_hbm, mixw_ref),
+    )
+    for load in late_loads:
+        load.start()
     cols = block(y, hid)
+    e_loads = gather_loads(
+        late + 1, (eg_hbm.at[0], gu.at[c, :, :part]), (eu_hbm.at[0], gu.at[c, :, part:])
+    ) + gather_loads(late + 2, (ed_hbm.at[0], ed.at[block(c, part), :]))
     loads = [
-        pltpu.make_async_copy(src, dst, w_sem.at[i])
-        for i, (src, dst) in enumerate(
+        gather_loads(1 + i, route)[0]
+        for i, route in enumerate(
             (
                 (ow_hbm, ow),
                 (dg_hbm.at[:, cols], dg),
@@ -690,9 +689,6 @@
             )
         )
     ]
-
-    for load in small_loads[:3]:
-        load.wait()
     resid = resid_ref[...].astype(F32)
     mean_sq = jnp.mean(resid * resid, axis=-1, keepdims=True)
     normed = (resid * lax.rsqrt(mean_sq + EPS) * first_gain_ref[...]).astype(BF16)
@@ -713,38 +709,25 @@
         )
         return (values * cosine + other * sine).astype(BF16).astype(F32)
 
-    for load in small_loads[3:]:
-        load.wait()
-
     def spot(plane, inner):
         return plane // CORES * INNER + inner
 
     own_spot = spot(z, x)
-    lane = lax.broadcasted_iota(jnp.int32, (seqs, route.shape[2]), 1)
-    table = jnp.zeros((seqs, route.shape[2]), F32)
-    for k in range(ids_ref.shape[0]):
-        wanted = column(ids_ref[k : k + 1, :])
-        table = table + jnp.where(lane == wanted, column(rw_ref[k : k + 1, :]), 0.0)
-
-    @pl.when(odd == 0)
-    def _():
-        route[own_spot] = table
-
-    query = jnp.zeros((seqs, qw.shape[1]), F32)
+    projected = jnp.zeros((seqs, qkv.shape[1]), F32)
     for i in range(Q_CHUNKS):
-        q_loads[i].wait()
-        query = query + dot(
-            normed[:, i * depth : (i + 1) * depth], qw[i * depth : (i + 1) * depth, :]
-        )
-    for load in q_loads[Q_CHUNKS:]:
-        load.wait()
-    keys_raw = dot(normed, kw[...])
-    values_raw = dot(normed, vw[...])
-    for load in loads:
+        deep = pl.ds(i * depth, depth)
+        pltpu.make_async_copy(qkv.at[deep, :], qkv.at[deep, :], local_sem.at[1 + i]).wait()
+        projected = projected + dot(normed[:, i * depth : (i + 1) * depth], qkv[deep, :])
+    query = projected[:, :inner]
+    keys_raw = projected[:, inner : inner + side]
+    values_raw = projected[:, inner + side :]
+    for load in e_loads + loads:
         load.start()
 
     groups, spots = cache.shape[1], cache.shape[2]
     share = query.shape[1] // LANES // groups
+    scale = QK_DIM**-0.5
+    lines = 2 * share
     lower = lax.broadcasted_iota(jnp.int32, (seqs, LANES), 1) < QK_DIM
     fresh = []
     for g in range(groups):
@@ -758,48 +741,36 @@
             head = rotate(query[:, at : at + LANES])
             pairs[g, :, j, :] = jnp.where(lower, head, 0.0)
             pairs[g, :, share + j, :] = jnp.where(lower, 0.0, head)
+        spread = (pairs[g] * scale).reshape(seqs * lines, LANES).astype(BF16)
+        turn_of = lax.broadcasted_iota(jnp.int32, spread.shape, 0) // lines % 2
+        asked[g, :, :LANES] = jnp.where(turn_of == 0, spread, jnp.zeros_like(spread))
+        asked[g, :, LANES:] = jnp.where(turn_of == 0, jnp.zeros_like(spread), spread)
 
     pl.semaphore_wait(barrier, n_ep * n_tp - 1)
 
     def push(index):
         where = (gu.at[c], ed.at[block(c, part), :])[index]
-        return remote(where, where, push_send.at[index], push_recv.at[index], (e, mate))
+        return remote(where, where, push_send.at[0], push_recv.at[index], (e, mate))
 
     def pushed(index):
         where = (gu.at[1 - c], ed.at[block(1 - c, part), :])[index]
-        remote(where, where, push_send.at[index], push_recv.at[index], (e, mate)).wait_recv()
-
-    for load in e_loads:
+        remote(where, where, push_send.at[0], push_recv.at[index], (e, mate)).wait_recv()
+
+    def beside(s, g, lanes):
+        return jnp.concatenate([cache[s, g, :, lanes], cache[s + 1, g, :, lanes]], axis=1)
+
+    for s in range(0, seqs, 2):
+        if s % bunch == 0:
+            cache_loads[s // bunch].wait()
+        for g in range(groups):
+            scores[g, s : s + 2] = lax.dot_general(
+                asked[g, s * lines : (s + 2) * lines, :],
+                beside(s, g, slice(0, LANES)),
+                (((1,), (1,)), ((), ())),
+                preferred_element_type=F32,
+            ).reshape(2, lines, spots)
+    for load in late_loads:
         load.wait()
-    push(0).start()
-    push(1).start()
-
-    def route_copy(mask):
-        where = route.at[own_spot]
-        return remote(
-            where, where, route_send.at[mask - 1], route_recv.at[own_spot], (flip(e, mask), t)
-        )
-
-    @pl.when(odd == 0)
-    def _():
-        for mask in range(1, n_ep):
-            route_copy(mask).start()
-
-    scale = QK_DIM**-0.5
-    lines = 2 * share
-    for s in range(seqs):
-        cache_loads[s].wait()
-        for g in range(groups):
-            both = pairs[g, s].astype(BF16)
-            scores[g, s] = (
-                lax.dot_general(
-                    both,
-                    cache[s, g, :, :LANES],
-                    (((1,), (1,)), ((), ())),
-                    preferred_element_type=F32,
-                )
-                * scale
-            )
     length = jnp.zeros((seqs, lines, 1), jnp.int32)
     which = lax.broadcasted_iota(jnp.int32, (seqs, lines, 1), 0)
     for s in range(seqs):
@@ -815,16 +786,21 @@
         raised = jnp.exp(masked - top)
         raised_new = jnp.exp(latest - top)
         total = jnp.sum(raised, axis=-1, keepdims=True) + raised_new
-        prob = raised / total
-        prob_new = jnp.broadcast_to(raised_new / total, (seqs, lines, LANES))
-        lam = jnp.zeros((lines, 1), F32)
+        lam = jnp.full((lines, 1), 1.0, F32)
         for j in range(share):
-            lam = jnp.where(line == j, lam_ref[g * share + j], lam)
-        scores[g] = prob - lam[None] * pltpu.roll(prob, share, 1)
-        new_weight = (prob_new - lam[None] * pltpu.roll(prob_new, share, 1)).astype(BF16).astype(F32)
+            lam = jnp.where(line == share + j, lam_ref[g * share + j], lam)
+        part_of = lam[None] / total
+        prob = raised * part_of
+        prob_new = jnp.broadcast_to(raised_new * part_of, (seqs, lines, LANES))
+        weights = (prob - pltpu.roll(prob, share, 1)).astype(BF16)
+        new_weight = (prob_new - pltpu.roll(prob_new, share, 1)).astype(BF16).astype(F32)
         fresh_part = new_weight * value[:, None, :]
-        for s in range(seqs):
-            mixed[g, s] = dot(scores[g, s].astype(BF16), cache[s, g, :, LANES:])
+        for s in range(0, seqs, 2):
+            both = dot(
+                weights[s : s + 2].reshape(2 * lines, spots), beside(s, g, slice(LANES, None))
+            )
+            mixed[g, s] = both[:lines, :LANES]
+            mixed[g, s + 1] = both[lines:, LANES:]
         whole = mixed[g] + fresh_part
         mean_sq = jnp.mean(whole * whole, axis=-1, keepdims=True)
         mixed[g] = whole * lax.rsqrt(mean_sq + EPS) * head_gain_ref[...][None]
@@ -836,20 +812,49 @@
         return remote(
             heads_ref,
             heads_all.at[mask - 1],
-            heads_send.at[mask - 1],
-            heads_recv.at[mask - 1],
+            heads_send.at[0],
+            heads_recv.at[mask // CORES],
             (e, flip(t, mask)),
         )
 
     for mask in range(n_tp - 1, 0, -1):
         heads_copy(mask).start()
+
+    for load in e_loads:
+        load.wait()
+    push(0).start()
+    push(1).start()
+
+    lane = lax.broadcasted_iota(jnp.int32, (seqs, route.shape[2]), 1)
+    table = jnp.zeros((seqs, route.shape[2]), F32)
+    for k in range(ids_ref.shape[0]):
+        wanted = column(ids_ref[k : k + 1, :])
+        table = table + jnp.where(lane == wanted, column(rw_ref[k : k + 1, :]), 0.0)
+
+    @pl.when(odd == 0)
+    def _():
+        route[own_spot] = table
+
+    def route_copy(mask):
+        where = route.at[own_spot]
+        return remote(
+            where, where, route_send.at[0], route_recv.at[0], (flip(e, mask), t)
+        )
+
+    @pl.when(odd == 0)
+    def _():
+        for mask in range(1, n_ep):
+            route_copy(mask).start()
+
 
     loads[0].wait()
     span = heads_ref.shape[1]
     total = dot(heads_ref[...], ow[block(t, span), :])
-    for mask in range(1, n_tp):
-        heads_copy(mask).wait_recv()
-        total = total + dot(heads_all[mask - 1], ow[block(flip(t, mask), span), :])
+    for far in range(n_tp // CORES):
+        batch = heads_all.at[pl.ds(0, 1) if far == 0 else pl.ds(far * CORES - 1, CORES)]
+        remote(batch, batch, heads_send.at[0], heads_recv.at[far], (e, t)).wait_recv()
+        for mask in range(max(far * CORES, 1), (far + 1) * CORES):
+            total = total + dot(heads_all[mask - 1], ow[block(flip(t, mask), span), :])
     own_cols = block(t, quarter)
     own_stream = (resid_ref[:, own_cols].astype(F32) + total).astype(BF16)
     mine[...] = own_stream
@@ -863,26 +868,18 @@
         dx, dy = around[step]
         there = (z * INNER + flip(x, dx), flip(y, dy) * CORES + keeper)
         return remote(
-            mine, at_spot(own_spot, t), first_send.at[step], stream_recv.at[own_spot, t], there
+            mine, at_spot(own_spot, t), chunk_send.at[0], group_recv.at[0, dx], there
         )
 
     def to_column(d):
         there = (flip(z, d) * INNER + x, y * CORES + keeper)
         return remote(
-            mine,
-            at_spot(own_spot, t),
-            first_send.at[len(around) + d],
-            stream_recv.at[own_spot, t],
-            there,
+            mine, at_spot(own_spot, t), chunk_send.at[0], climb_recv.at[d // CORES, c], there
         )
 
     def to_mate():
         return remote(
-            mine,
-            at_spot(own_spot, t),
-            first_send.at[len(around)],
-            stream_recv.at[own_spot, t],
-            (e, mate),
+            mine, at_spot(own_spot, t), chunk_send.at[0], climb_recv.at[0, c], (e, mate)
         )
 
     for d in range(planes - 1, 0, -1):
@@ -903,28 +900,24 @@
     def plane_of(i):
         return flip(near, 2 * i)
 
-    def arrived(where, owner):
-        spot_ref = at_spot(where, owner)
-        remote(
-            spot_ref, spot_ref, first_send.at[0], stream_recv.at[where, owner], (e, t)
-        ).wait_recv()
+    def arrived(i, core):
+        where = at_spot(spot(plane_of(i), x), y * CORES + core)
+        remote(where, where, chunk_send.at[0], climb_recv.at[i, core], (e, t)).wait_recv()
 
     def forward(i, core, step):
         dx, dy = around[step]
-        owner = y * CORES + core
-        where = spot(plane_of(i), x)
-        spot_ref = at_spot(where, owner)
+        where = at_spot(spot(plane_of(i), x), y * CORES + core)
         return remote(
-            spot_ref,
-            spot_ref,
-            second_send.at[i, core, step],
-            stream_recv.at[where, owner],
+            where,
+            where,
+            chunk_send.at[0],
+            group_recv.at[i, dx],
             (z * INNER + flip(x, dx), flip(y, dy) * CORES + c),
         )
 
     def relay(i):
         for core in range(CORES):
-            arrived(spot(plane_of(i), x), y * CORES + core)
+            arrived(i, core)
             for step in range(len(around)):
                 forward(i, core, step).start()
 
@@ -937,19 +930,15 @@
 
             @pl.when(odd == 0)
             def _():
-                arrived(own_spot, mate)
+                arrived(0, 1 - c)
         else:
             relay(i)
 
     def normalise(i):
-        for inner in (0, 1):
-            where = spot(plane_of(i), flip(x, inner))
-            for core in range(CORES):
-                arrived(where, flip(y, 1) * CORES + core)
-            if inner:
-                for core in range(CORES):
-                    arrived(where, y * CORES + core)
-            rows = block(where, seqs)
+        for inner in range(INNER):
+            rows = block(spot(plane_of(i), flip(x, inner)), seqs)
+            came = stream.at[rows, :] if inner else stream.at[rows, block(flip(y, 1), CORES * quarter)]
+            remote(came, came, chunk_send.at[0], group_recv.at[i, inner], (e, t)).wait_recv()
             values = stream[rows, :].astype(F32)
             mean_sq = jnp.mean(values * values, axis=-1, keepdims=True)
             scaled = (values * lax.rsqrt(mean_sq + EPS) * gain_ref[...]).astype(BF16)
@@ -962,23 +951,17 @@
     for i in range(turns):
         normalise(i)
 
-    for i in range(turns):
-        for inner in range(INNER):
-            where = spot(plane_of(i), inner)
-
-            def route_wait(where=where):
-                spot_ref = route.at[where]
-                remote(
-                    spot_ref, spot_ref, route_send.at[0], route_recv.at[where], (e, t)
-                ).wait_recv()
-
-            if i == 0:
-
-                @pl.when(jnp.logical_or(odd == 1, inner != x))
-                def _():
-                    route_wait()
-            else:
-                route_wait()
+    def route_wait(count):
+        where = route.at[pl.ds(0, count)]
+        remote(where, where, route_send.at[0], route_recv.at[0], (e, t)).wait_recv()
+
+    @pl.when(odd == 0)
+    def _():
+        route_wait(route.shape[0] - 1)
+
+    @pl.when(odd == 1)
+    def _():
+        route_wait(route.shape[0])
 
     rows_all = ffn.shape[0]
     pushed(0)
@@ -1001,29 +984,29 @@
         keepdims=True,
     )
 
-    def leave(i, dy, core, step):
-        dx = around[step][0]
+    def leave(i, core, step):
+        dx, dy = around[step]
         where = spot(plane_of(i), flip(x, dx))
         return remote(
-            leaving.at[dy, core, block(where, seqs), :],
+            leaving.at[dy, block(where, seqs), pl.ds(core * quarter, quarter)],
             plane_in.at[i, core, step],
-            plane_send.at[i, core, step],
-            plane_recv.at[i, core, step],
+            chunk_send.at[0],
+            plane_recv.at[i, core],
             (z * INNER + flip(x, dx), flip(y, dy) * CORES + c),
         )
 
     order = range(turns - 1, -1, -1)
     for dy in (1, 0):
-        for core in range(CORES):
-            cols = block(flip(y, dy) * CORES + core, quarter)
-            total = mix[:, :1] * dot(dh[...], dd[:, cols]) + weight * dot(eh[...], ed[:, cols])
-            leaving[dy, core] = total.astype(BF16)
-            if not dy:
-                kept[core] = total
-            for i in order:
+        cols = block(flip(y, dy), CORES * quarter)
+        total = mix[:, :1] * dot(dh[...], dd[:, cols]) + weight * dot(eh[...], ed[:, cols])
+        leaving[dy] = total.astype(BF16)
+        if not dy:
+            kept[...] = total
+        for i in order:
+            for core in range(CORES):
                 for step in range(len(around)):
                     if around[step][1] == dy:
-                        leave(i, dy, core, step).start()
+                        leave(i, core, step).start()
 
     def own_plane(i):
         return jnp.logical_and(odd == 0, i == 0)
@@ -1032,8 +1015,8 @@
         return remote(
             column_out.at[i, core],
             column_in.at[odd + 2 * i],
-            column_send.at[i, core],
-            column_recv.at[odd + 2 * i],
+            chunk_send.at[0],
+            column_recv.at[0],
             (plane_of(i) * INNER + x, y * CORES + core),
         )
 
@@ -1042,9 +1025,10 @@
 
     for i in order:
         for core in range(CORES):
-            gathered = kept[core, block(spot(plane_of(i), x), seqs), :]
+            gathered = kept[block(spot(plane_of(i), x), seqs), core * quarter : (core + 1) * quarter]
+            came = plane_in.at[i, core]
+            remote(came, came, chunk_send.at[0], plane_recv.at[i, core], (e, t)).wait_recv()
             for step in range(len(around)):
-                leave(i, around[step][1], core, step).wait_recv()
                 gathered = gathered + plane_in[i, core, step].astype(F32)
             column_out[i, core] = gathered.astype(BF16)
 
@@ -1052,59 +1036,43 @@
             def _(i=i, core=core):
                 climb(i, core).start()
 
-    def took(d):
-        where = column_in.at[d]
-        remote(where, where, column_send.at[0, 0], column_recv.at[d], (e, t)).wait_recv()
+    def took(start):
+        where = column_in.at[pl.ds(start, planes - start)]
+        remote(where, where, chunk_send.at[0], column_recv.at[0], (e, t)).wait_recv()
 
     @pl.when(odd == 0)
     def _():
         column_in[0] = column_out[0, c]
+        took(1)
 
     @pl.when(odd == 1)
     def _():
         took(0)
 
-    for d in range(1, planes):
-        took(d)
     out_ref[...] = (
         own_stream.astype(F32) + jnp.sum(column_in[...].astype(F32), axis=0)
     ).astype(BF16)
 
     push(0).wait_send()
     push(1).wait_send()
-    for mask in range(1, n_tp):
-        heads_copy(mask).wait_send()
+    remote(heads_all, heads_all, heads_send.at[0], heads_recv.at[0], (e, t)).wait_send()
+
+    def drained(count):
+        where = ow.at[pl.ds(0, count * seqs), :]
+        remote(where, where, chunk_send.at[0], column_recv.at[0], (e, t)).wait_send()
+
+    hops = len(around)
+    always = planes - 1 + hops + 2 * turns * CORES * hops + turns * CORES
 
     @pl.when(odd == 0)
     def _():
         for mask in range(1, n_ep):
             route_copy(mask).wait_send()
-
-    for d in range(1, planes):
-        to_column(d).wait_send()
-    for step in range(len(around)):
-        to_plane(step).wait_send()
+        drained(always - CORES * hops - 1)
 
     @pl.when(odd == 1)
     def _():
-        to_mate().wait_send()
-
-    for i in range(turns):
-        for core in range(CORES):
-            for step in range(len(around)):
-
-                def forwarded(i=i, core=core, step=step):
-                    forward(i, core, step).wait_send()
-
-                if i == 0:
-                    pl.when(odd == 1)(forwarded)
-                else:
-                    forwarded()
-                leave(i, around[step][1], core, step).wait_send()
-
-            @pl.when(jnp.logical_not(stays(i, core)))
-            def _(i=i, core=core):
-                climb(i, core).wait_send()
+        drained(always + 1)
 
 
 def near_call(n_ep, n_tp, arrays):
@@ -1164,11 +1132,10 @@
             pltpu.VMEM((1, width), F32),
             pltpu.VMEM((topk, seqs), jnp.int32),
             pltpu.VMEM((topk, seqs), F32),
-            pltpu.VMEM(query_weight.shape, BF16),
-            pltpu.VMEM(key_weight.shape, BF16),
-            pltpu.VMEM(value_weight.shape, BF16),
+            pltpu.VMEM((width, inner + key_weight.shape[1] + value_weight.shape[1]), BF16),
             pltpu.VMEM(kv_cache.shape, BF16),
             pltpu.VMEM((groups, seqs, 2 * share, LANES), F32),
+            pltpu.VMEM((groups, seqs * 2 * share, 2 * LANES), BF16),
             pltpu.VMEM((groups, seqs, 2 * share, spots), F32),
             pltpu.VMEM((groups, seqs, 2 * share, LANES), F32),
             pltpu.VMEM((seqs, inner), BF16),
@@ -1186,29 +1153,23 @@
             pltpu.VMEM((blocks, seqs, lanes), F32),
             pltpu.VMEM((rows, CORES * part), BF16),
             pltpu.VMEM((rows, hid), BF16),
-            pltpu.VMEM((2, CORES, rows, quarter), BF16),
-            pltpu.VMEM((CORES, rows, quarter), F32),
+            pltpu.VMEM((2, rows, CORES * quarter), BF16),
+            pltpu.VMEM((rows, CORES * quarter), F32),
             pltpu.VMEM((turns, CORES, 3, seqs, quarter), BF16),
             pltpu.VMEM((turns, CORES, seqs, quarter), BF16),
             pltpu.VMEM((n_ep // INNER, seqs, quarter), BF16),
-            dma((9,)),
-            dma((Q_CHUNKS + 2,)),
-            dma((seqs,)),
-            dma((4,)),
-            dma((3,)),
+            dma((Q_CHUNKS + CACHE_CHUNKS + 4,)),
+            dma((1,)),
             dma((2,)),
-            dma((2,)),
-            dma((n_ep - 1,)),
-            dma((blocks,)),
-            dma((n_tp - 1,)),
-            dma((n_tp - 1,)),
-            dma((3 + n_ep // INNER,)),
-            dma((turns, CORES, 3)),
-            dma((blocks, n_tp)),
-            dma((turns, CORES, 3)),
-            dma((turns, CORES, 3)),
+            dma((1,)),
+            dma((1,)),
+            dma((1,)),
+            dma((n_tp // CORES,)),
+            dma((1,)),
             dma((turns, CORES)),
-            dma((n_ep // INNER,)),
+            dma((turns, INNER)),
+            dma((turns, CORES)),
+            dma((1,)),
         ],
         compiler_params=pltpu.CompilerParams(
             collective_id=0, has_side_effects=True, vmem_limit_bytes=36 * 1024 * 1024

time: 33.3 us -> 30.4 us (0.913)
  Pallas kernels: 31.3 us -> 28.4 us
    pallas_call x1, Pallas kernels: 31.3 us -> 28.4 us  [near_call(): pl.pallas_call(functools.partial(near_kernel, n_ep, n_tp), out_shape=(jax...]
where the time goes in v2:
time: 30.4 us; the launch traced here: 30.3 us
  Pallas kernels  28.4 us (93%)
  local copies, waits for them, and re-layouts  1.21 us (4%)
  between operations  0.65 us (2%)
    pallas_call x1, Pallas kernels, near_call(): pl.pallas_call(functools.partial(near_kernel, n_ep, n_tp), out_shape=(jax...  28.4 us
    unnamed x2, local copies, waits for them, and re-layouts  1.21 us

profile of v2, /device:TPU:0, one launch (start us, length us, event | category | flops | bytes accessed | tf_op | source)
XLA Modules:
  0.0 30.3 jit_solution(13981227086496092816)
XLA Ops:
  0.6 28.4 %shard_map.203 = (bf16[16,512]{1,0:T(8,128)(2,1)S(1)}, bf16[16,256]{1,0:T(8,128)(2,1)S(1)}) custom-call(s32[16]{0:T(128)} %lengths_hbm.1, f32[4]{0:T(128)} %lam_hbm.1, bf16[16,2048]{1,0:T(8,128)(2,1)} %resid_hbm.1, f32[1,2048]{1,0:T(1,128)} %bitcast.8, f32[1,128]{1,0:T(1,128)} %bitcast.13, f32[1,2048]{1,0:T(1,128)} %bitcast.9, f32[1,2048]{1,0:T(1,128)} %bitcast.10, ...), custom_call_target="tpu_custom_call" | custom-call | tf_op jit(solution)/shard_map/pallas_call | solution.py:1117
  29.1 0.6 %copy.24 = bf16[16,512]{1,0:T(8,128)(2,1)} copy(bf16[16,512]{1,0:T(8,128)(2,1)S(1)} %get-tuple-element.8) | data formatting | bytes 32768
  29.7 0.6 %copy.25 = bf16[16,1,256]{2,0,1:T(8,128)(2,1)} copy(bf16[16,1,256]{2,0,1:T(8,128)(2,1)S(1)} %bitcast.7) | data formatting | bytes 16384

commit v3 on v2

--- a/solution.py
+++ b/solution.py
@@ -17,6 +17,7 @@
 Q_CHUNKS = 4
 INNER = 2
 CORES = 2
+RELAY = 1
 CACHE_CHUNKS = 4
 
 
@@ -583,7 +584,6 @@
     mine,
     stream,
     ffn,
-    mix,
     route,
     eh,
     dh,
@@ -745,8 +745,6 @@
         turn_of = lax.broadcasted_iota(jnp.int32, spread.shape, 0) // lines % 2
         asked[g, :, :LANES] = jnp.where(turn_of == 0, spread, jnp.zeros_like(spread))
         asked[g, :, LANES:] = jnp.where(turn_of == 0, jnp.zeros_like(spread), spread)
-
-    pl.semaphore_wait(barrier, n_ep * n_tp - 1)
 
     def push(index):
         where = (gu.at[c], ed.at[block(c, part), :])[index]
@@ -817,6 +815,7 @@
             (e, flip(t, mask)),
         )
 
+    pl.semaphore_wait(barrier, n_ep * n_tp - 1)
     for mask in range(n_tp - 1, 0, -1):
         heads_copy(mask).start()
 
@@ -860,30 +859,44 @@
     mine[...] = own_stream
 
     around = ((1, 1), (1, 0), (0, 1))
-
-    def at_spot(where, owner):
-        return stream.at[block(where, seqs), block(owner, quarter)]
+    last = turns - 1
+    edge = jnp.logical_or(z == 0, z == planes - 1)
+    far = jnp.logical_and(edge, odd == 1)
+
+    def chunk(group, owner):
+        return stream.at[block(group, seqs), block(owner, quarter)]
 
     def to_plane(step):
         dx, dy = around[step]
         there = (z * INNER + flip(x, dx), flip(y, dy) * CORES + keeper)
         return remote(
-            mine, at_spot(own_spot, t), chunk_send.at[0], group_recv.at[0, dx], there
+            mine, chunk(e, t), chunk_send.at[0], group_recv.at[z // CORES, dx], there
         )
 
     def to_column(d):
-        there = (flip(z, d) * INNER + x, y * CORES + keeper)
+        core = jnp.where(z == planes - 1, keeper, RELAY) if d == planes - 1 else RELAY
+        there = (flip(z, d) * INNER + x, y * CORES + core)
+        return remote(mine, chunk(e, t), chunk_send.at[0], climb_recv.at[z, c], there)
+
+    def to_mate():
+        return remote(mine, chunk(e, t), chunk_send.at[0], climb_recv.at[z, c], (e, mate))
+
+    def to_far(step):
+        dx, dy = around[step]
+        there = (flip(z, planes - 1) * INNER + flip(x, dx), flip(y, dy) * CORES + keeper)
         return remote(
-            mine, at_spot(own_spot, t), chunk_send.at[0], climb_recv.at[d // CORES, c], there
-        )
-
-    def to_mate():
-        return remote(
-            mine, at_spot(own_spot, t), chunk_send.at[0], climb_recv.at[0, c], (e, mate)
-        )
-
-    for d in range(planes - 1, 0, -1):
+            mine, chunk(e, t), chunk_send.at[0], group_recv.at[z // CORES, dx], there
+        )
+
+    for d in range(planes - 2, 0, -1):
         to_column(d).start()
+
+    @pl.when(z == planes - 1)
+    def _():
+        for step in range(len(around)):
+            to_far(step).start()
+
+    to_column(planes - 1).start()
     for step in range(len(around)):
         to_plane(step).start()
 
@@ -893,61 +906,76 @@
 
     @pl.when(odd == 0)
     def _():
-        stream[block(own_spot, seqs), own_cols] = own_stream
+        stream[block(e, seqs), own_cols] = own_stream
 
     near = z + odd * (1 - 2 * (z % 2))
 
     def plane_of(i):
         return flip(near, 2 * i)
 
-    def arrived(i, core):
-        where = at_spot(spot(plane_of(i), x), y * CORES + core)
-        remote(where, where, chunk_send.at[0], climb_recv.at[i, core], (e, t)).wait_recv()
-
-    def forward(i, core, step):
+    def arrived(plane, core):
+        where = chunk(plane * INNER + x, y * CORES + core)
+        remote(where, where, chunk_send.at[0], climb_recv.at[plane, core], (e, t)).wait_recv()
+
+    def forward(plane, core, step):
         dx, dy = around[step]
-        where = at_spot(spot(plane_of(i), x), y * CORES + core)
+        where = chunk(plane * INNER + x, y * CORES + core)
         return remote(
             where,
             where,
             chunk_send.at[0],
-            group_recv.at[i, dx],
-            (z * INNER + flip(x, dx), flip(y, dy) * CORES + c),
-        )
-
-    def relay(i):
-        for core in range(CORES):
-            arrived(i, core)
-            for step in range(len(around)):
-                forward(i, core, step).start()
-
-    def gather(i):
-        if i == 0:
-
-            @pl.when(odd == 1)
-            def _():
-                relay(0)
-
-            @pl.when(odd == 0)
-            def _():
-                arrived(0, 1 - c)
-        else:
-            relay(i)
+            group_recv.at[plane // CORES, dx],
+            (z * INNER + flip(x, dx), flip(y, dy) * CORES + plane % CORES),
+        )
+
+    def hand_over(plane, core):
+        where = chunk(plane * INNER + x, y * CORES + core)
+        return remote(where, where, chunk_send.at[0], climb_recv.at[plane, core], (e, mate))
+
+    @pl.when(c == RELAY)
+    def _():
+        for plane in range(planes):
+            passes = plane != z
+            if plane == planes - 1:
+                passes = jnp.logical_and(passes, z != 0)
+
+            @pl.when(passes)
+            def _(plane=plane):
+                for core in range(CORES):
+                    arrived(plane, core)
+                    for step in range(len(around)):
+                        forward(plane, core, step).start()
+                    if plane % CORES != RELAY:
+                        hand_over(plane, core).start()
 
     def normalise(i):
+        plane = CORES * i + c
+
+        @pl.when(plane == z)
+        def _():
+            arrived(plane, 1 - c)
+
+        leapt = jnp.logical_and(plane == planes - 1, z == 0)
+
+        @pl.when(jnp.logical_and(plane != z, jnp.logical_or(c != RELAY, leapt)))
+        def _():
+            for core in range(CORES):
+                arrived(plane, core)
+
         for inner in range(INNER):
-            rows = block(spot(plane_of(i), flip(x, inner)), seqs)
-            came = stream.at[rows, :] if inner else stream.at[rows, block(flip(y, 1), CORES * quarter)]
-            remote(came, came, chunk_send.at[0], group_recv.at[i, inner], (e, t)).wait_recv()
-            values = stream[rows, :].astype(F32)
+            group = plane * INNER + flip(x, inner)
+            came = stream.at[
+                block(group, seqs),
+                pl.ds(0, width) if inner else block(flip(y, 1), CORES * quarter),
+            ]
+            remote(
+                came, came, chunk_send.at[0], group_recv.at[plane // CORES, inner], (e, t)
+            ).wait_recv()
+            values = stream[block(group, seqs), :].astype(F32)
             mean_sq = jnp.mean(values * values, axis=-1, keepdims=True)
             scaled = (values * lax.rsqrt(mean_sq + EPS) * gain_ref[...]).astype(BF16)
-            ffn[rows, :] = scaled
-            inside = jnp.sum(scaled.astype(F32) * mixw_ref[...], axis=-1, keepdims=True)
-            mix[rows, :] = jnp.broadcast_to(jax.nn.sigmoid(inside), (seqs, LANES))
-
-    for i in range(turns):
-        gather(i)
+            ffn[block(spot(plane, flip(x, inner)), seqs), :] = scaled
+
     for i in range(turns):
         normalise(i)
 
@@ -966,23 +994,29 @@
     rows_all = ffn.shape[0]
     pushed(0)
     pushed(1)
-    for load in loads[1:3]:
+    for load in loads[1:]:
         load.wait()
     a = ffn[...]
+    dh[...] = (jax.nn.silu(dot(a, dg[...])) * dot(a, du[...])).astype(BF16)
     for core in range(CORES):
         both = dot(a, gu[core])
         eh[:, core * part : (core + 1) * part] = (
             jax.nn.silu(both[:, :part]) * both[:, part:]
         ).astype(BF16)
-    dh[...] = (jax.nn.silu(dot(a, dg[...])) * dot(a, du[...])).astype(BF16)
-    loads[3].wait()
-
+    blend = jax.nn.sigmoid(jnp.sum(a.astype(F32) * mixw_ref[...], axis=-1, keepdims=True))
     lanes = lax.broadcasted_iota(jnp.int32, (rows_all, route.shape[2]), 1)
     weight = jnp.sum(
         jnp.where(lanes == e, route[...].reshape(rows_all, route.shape[2]), 0.0),
         axis=1,
         keepdims=True,
     )
+    half = CORES * quarter
+    for dy in (1, 0):
+        cols = block(flip(y, dy), half)
+        total = blend * dot(dh[...], dd[:, cols]) + weight * dot(eh[...], ed[:, cols])
+        leaving[dy] = total.astype(BF16)
+        if not dy:
+            kept[...] = total
 
     def leave(i, core, step):
         dx, dy = around[step]
@@ -995,18 +1029,38 @@
             (z * INNER + flip(x, dx), flip(y, dy) * CORES + c),
         )
 
+    def leap(core, step):
+        dx, dy = around[step] if step < len(around) else (0, 0)
+        where = spot(plane_of(last), flip(x, dx))
+        return remote(
+            leaving.at[dy, block(where, seqs), pl.ds(core * quarter, quarter)],
+            column_in.at[planes - 1 + (step + 1) % (len(around) + 1)],
+            chunk_send.at[0],
+            column_recv.at[0],
+            (plane_of(last) * INNER + flip(x, dx), flip(y, dy) * CORES + core),
+        )
+
     order = range(turns - 1, -1, -1)
     for dy in (1, 0):
-        cols = block(flip(y, dy), CORES * quarter)
-        total = mix[:, :1] * dot(dh[...], dd[:, cols]) + weight * dot(eh[...], ed[:, cols])
-        leaving[dy] = total.astype(BF16)
-        if not dy:
-            kept[...] = total
+        steps = [step for step in range(len(around)) if around[step][1] == dy]
+
+        @pl.when(far)
+        def _():
+            for step in steps + [len(around)] * (1 - dy):
+                for core in range(CORES):
+                    leap(core, step).start()
+
         for i in order:
-            for core in range(CORES):
-                for step in range(len(around)):
-                    if around[step][1] == dy:
+
+            def depart(i=i):
+                for core in range(CORES):
+                    for step in steps:
                         leave(i, core, step).start()
+
+            if i == last:
+                pl.when(jnp.logical_not(far))(depart)
+            else:
+                depart()
 
     def own_plane(i):
         return jnp.logical_and(odd == 0, i == 0)
@@ -1023,7 +1077,7 @@
     def stays(i, core):
         return jnp.logical_and(own_plane(i), c == core)
 
-    for i in order:
+    def rise(i):
         for core in range(CORES):
             gathered = kept[block(spot(plane_of(i), x), seqs), core * quarter : (core + 1) * quarter]
             came = plane_in.at[i, core]
@@ -1036,22 +1090,41 @@
             def _(i=i, core=core):
                 climb(i, core).start()
 
-    def took(start):
-        where = column_in.at[pl.ds(start, planes - start)]
+    for i in order:
+        if i == last:
+
+            @pl.when(jnp.logical_not(far))
+            def _(i=i):
+                rise(i)
+        else:
+            rise(i)
+
+    def took(start, stop):
+        where = column_in.at[pl.ds(start, stop - start)]
         remote(where, where, chunk_send.at[0], column_recv.at[0], (e, t)).wait_recv()
 
     @pl.when(odd == 0)
     def _():
         column_in[0] = column_out[0, c]
-        took(1)
-
-    @pl.when(odd == 1)
+
+    def finish(stop):
+        for parity in range(2):
+
+            @pl.when(odd == parity)
+            def _(parity=parity):
+                took(1 - parity, stop)
+
+        out_ref[...] = (
+            own_stream.astype(F32) + jnp.sum(column_in[:stop].astype(F32), axis=0)
+        ).astype(BF16)
+
+    @pl.when(edge)
     def _():
-        took(0)
-
-    out_ref[...] = (
-        own_stream.astype(F32) + jnp.sum(column_in[...].astype(F32), axis=0)
-    ).astype(BF16)
+        finish(planes + len(around))
+
+    @pl.when(jnp.logical_not(edge))
+    def _():
+        finish(planes)
 
     push(0).wait_send()
     push(1).wait_send()
@@ -1062,17 +1135,23 @@
         remote(where, where, chunk_send.at[0], column_recv.at[0], (e, t)).wait_send()
 
     hops = len(around)
-    always = planes - 1 + hops + 2 * turns * CORES * hops + turns * CORES
-
     @pl.when(odd == 0)
     def _():
         for mask in range(1, n_ep):
             route_copy(mask).wait_send()
-        drained(always - CORES * hops - 1)
-
-    @pl.when(odd == 1)
-    def _():
-        drained(always + 1)
+
+    for level in range(planes):
+        for core in range(CORES):
+            count = planes - 1 + hops + turns * CORES * (hops + 1)
+            count += hops if level == planes - 1 else 0
+            count += 1 if (level + core) % CORES else -1
+            for plane in range(planes) if core == RELAY else ():
+                if plane != level and plane - level != planes - 1:
+                    count += CORES * (hops + (plane % CORES != RELAY))
+
+            @pl.when(jnp.logical_and(z == level, c == core))
+            def _(count=count):
+                drained(count)
 
 
 def near_call(n_ep, n_tp, arrays):
@@ -1147,9 +1226,8 @@
             pltpu.VMEM((hid, width), BF16),
             pltpu.VMEM((n_tp - 1, seqs, inner), BF16),
             pltpu.VMEM((seqs, quarter), BF16),
+            pltpu.VMEM((n_ep * seqs, width), BF16),
             pltpu.VMEM((rows, width), BF16),
-            pltpu.VMEM((rows, width), BF16),
-            pltpu.VMEM((rows, LANES), F32),
             pltpu.VMEM((blocks, seqs, lanes), F32),
             pltpu.VMEM((rows, CORES * part), BF16),
             pltpu.VMEM((rows, hid), BF16),
@@ -1157,7 +1235,7 @@
             pltpu.VMEM((rows, CORES * quarter), F32),
             pltpu.VMEM((turns, CORES, 3, seqs, quarter), BF16),
             pltpu.VMEM((turns, CORES, seqs, quarter), BF16),
-            pltpu.VMEM((n_ep // INNER, seqs, quarter), BF16),
+            pltpu.VMEM((n_ep // INNER + 3, seqs, quarter), BF16),
             dma((Q_CHUNKS + CACHE_CHUNKS + 4,)),
             dma((1,)),
             dma((2,)),
@@ -1166,7 +1244,7 @@
             dma((1,)),
             dma((n_tp // CORES,)),
             dma((1,)),
-            dma((turns, CORES)),
+            dma((n_ep // INNER, CORES)),
             dma((turns, INNER)),
             dma((turns, CORES)),
             dma((1,)),

time: 30.4 us -> 28.6 us (0.941)
  Pallas kernels: 28.4 us -> 26.6 us
    pallas_call x1, Pallas kernels: 28.4 us -> 26.6 us  [near_call(): pl.pallas_call(functools.partial(near_kernel, n_ep, n_tp), out_shape=(jax...]
where the time goes in v3:
time: 28.6 us; the launch traced here: 28.5 us
  Pallas kernels  26.6 us (93%)
  local copies, waits for them, and re-layouts  1.21 us (4%)
  between operations  0.65 us (2%)
    pallas_call x1, Pallas kernels, near_call(): pl.pallas_call(functools.partial(near_kernel, n_ep, n_tp), out_shape=(jax...  26.6 us
    unnamed x2, local copies, waits for them, and re-layouts  1.21 us

profile of v3, /device:TPU:0, one launch (start us, length us, event | category | flops | bytes accessed | tf_op | source)
XLA Modules:
  0.0 28.5 jit_solution(2384292982535292137)
XLA Ops:
  0.6 26.6 %shard_map.203 = (bf16[16,512]{1,0:T(8,128)(2,1)S(1)}, bf16[16,256]{1,0:T(8,128)(2,1)S(1)}) custom-call(s32[16]{0:T(128)} %lengths_hbm.1, f32[4]{0:T(128)} %lam_hbm.1, bf16[16,2048]{1,0:T(8,128)(2,1)} %resid_hbm.1, f32[1,2048]{1,0:T(1,128)} %bitcast.8, f32[1,128]{1,0:T(1,128)} %bitcast.13, f32[1,2048]{1,0:T(1,128)} %bitcast.9, f32[1,2048]{1,0:T(1,128)} %bitcast.10, ...), custom_call_target="tpu_custom_call" | custom-call | tf_op jit(solution)/shard_map/pallas_call | solution.py:1196
  27.3 0.6 %copy.24 = bf16[16,512]{1,0:T(8,128)(2,1)} copy(bf16[16,512]{1,0:T(8,128)(2,1)S(1)} %get-tuple-element.8) | data formatting | bytes 32768
  27.9 0.6 %copy.25 = bf16[16,1,256]{2,0,1:T(8,128)(2,1)} copy(bf16[16,1,256]{2,0,1:T(8,128)(2,1)S(1)} %bitcast.7) | data formatting | bytes 16384

commit v4 on v3

--- a/solution.py
+++ b/solution.py
@@ -757,51 +757,66 @@
     def beside(s, g, lanes):
         return jnp.concatenate([cache[s, g, :, lanes], cache[s + 1, g, :, lanes]], axis=1)
 
-    for s in range(0, seqs, 2):
-        if s % bunch == 0:
-            cache_loads[s // bunch].wait()
+    place = lax.broadcasted_iota(jnp.int32, (bunch, lines, spots), 2)
+    line = lax.broadcasted_iota(jnp.int32, (lines, 1), 0)
+
+    def score(start):
+        for s in range(start, start + bunch, 2):
+            for g in range(groups):
+                scores[g, s : s + 2] = lax.dot_general(
+                    asked[g, s * lines : (s + 2) * lines, :],
+                    beside(s, g, slice(0, LANES)),
+                    (((1,), (1,)), ((), ())),
+                    preferred_element_type=F32,
+                ).reshape(2, lines, spots)
+
+    def attend(start):
+        stop = start + bunch
+        length = jnp.zeros((bunch, lines, 1), jnp.int32)
+        which = lax.broadcasted_iota(jnp.int32, (bunch, lines, 1), 0)
+        for s in range(bunch):
+            length = jnp.where(which == s, lengths_ref[start + s], length)
+        valid = place < length
         for g in range(groups):
-            scores[g, s : s + 2] = lax.dot_general(
-                asked[g, s * lines : (s + 2) * lines, :],
-                beside(s, g, slice(0, LANES)),
-                (((1,), (1,)), ((), ())),
-                preferred_element_type=F32,
-            ).reshape(2, lines, spots)
-    for load in late_loads:
-        load.wait()
-    length = jnp.zeros((seqs, lines, 1), jnp.int32)
-    which = lax.broadcasted_iota(jnp.int32, (seqs, lines, 1), 0)
-    for s in range(seqs):
-        length = jnp.where(which == s, lengths_ref[s], length)
-    place = lax.broadcasted_iota(jnp.int32, (seqs, lines, spots), 2)
-    valid = place < length
-    line = lax.broadcasted_iota(jnp.int32, (lines, 1), 0)
+            key, value = (half[start:stop] for half in fresh[g])
+            latest = jnp.sum(pairs[g, start:stop] * key[:, None, :], axis=-1, keepdims=True) * scale
+            masked = jnp.where(valid, scores[g, start:stop], -jnp.inf)
+            top = jnp.maximum(jnp.max(masked, axis=-1, keepdims=True), latest)
+            raised = jnp.exp(masked - top)
+            raised_new = jnp.exp(latest - top)
+            total = jnp.sum(raised, axis=-1, keepdims=True) + raised_new
+            lam = jnp.full((lines, 1), 1.0, F32)
+            for j in range(share):
+                lam = jnp.where(line == share + j, lam_ref[g * share + j], lam)
+            part_of = lam[None] / total
+            prob = raised * part_of
+            prob_new = jnp.broadcast_to(raised_new * part_of, (bunch, lines, LANES))
+            weights = (prob - pltpu.roll(prob, share, 1)).astype(BF16)
+            new_weight = (
+                (prob_new - pltpu.roll(prob_new, share, 1)).astype(BF16).astype(F32)
+            )
+            fresh_part = new_weight * value[:, None, :]
+            for s in range(0, bunch, 2):
+                both = dot(
+                    weights[s : s + 2].reshape(2 * lines, spots),
+                    beside(start + s, g, slice(LANES, None)),
+                )
+                mixed[g, start + s] = both[:lines, :LANES]
+                mixed[g, start + s + 1] = both[lines:, LANES:]
+            whole = mixed[g, start:stop] + fresh_part
+            mean_sq = jnp.mean(whole * whole, axis=-1, keepdims=True)
+            mixed[g, start:stop] = whole * lax.rsqrt(mean_sq + EPS) * head_gain_ref[...][None]
+
+    for i in range(CACHE_CHUNKS):
+        if i == CACHE_CHUNKS - 1:
+            for load in late_loads:
+                load.wait()
+        cache_loads[i].wait()
+        score(i * bunch)
+        if i == CACHE_CHUNKS - 1:
+            for k in range(CACHE_CHUNKS):
+                attend(k * bunch)
     for g in range(groups):
-        key, value = fresh[g]
-        latest = jnp.sum(pairs[g] * key[:, None, :], axis=-1, keepdims=True) * scale
-        masked = jnp.where(valid, scores[g], -jnp.inf)
-        top = jnp.maximum(jnp.max(masked, axis=-1, keepdims=True), latest)
-        raised = jnp.exp(masked - top)
-        raised_new = jnp.exp(latest - top)
-        total = jnp.sum(raised, axis=-1, keepdims=True) + raised_new
-        lam = jnp.full((lines, 1), 1.0, F32)
-        for j in range(share):
-            lam = jnp.where(line == share + j, lam_ref[g * share + j], lam)
-        part_of = lam[None] / total
-        prob = raised * part_of
-        prob_new = jnp.broadcast_to(raised_new * part_of, (seqs, lines, LANES))
-        weights = (prob - pltpu.roll(prob, share, 1)).astype(BF16)
-        new_weight = (prob_new - pltpu.roll(prob_new, share, 1)).astype(BF16).astype(F32)
-        fresh_part = new_weight * value[:, None, :]
-        for s in range(0, seqs, 2):
-            both = dot(
-                weights[s : s + 2].reshape(2 * lines, spots), beside(s, g, slice(LANES, None))
-            )
-            mixed[g, s] = both[:lines, :LANES]
-            mixed[g, s + 1] = both[lines:, LANES:]
-        whole = mixed[g] + fresh_part
-        mean_sq = jnp.mean(whole * whole, axis=-1, keepdims=True)
-        mixed[g] = whole * lax.rsqrt(mean_sq + EPS) * head_gain_ref[...][None]
         for j in range(share):
             at = (g * share + j) * LANES
             heads_ref[:, at : at + LANES] = mixed[g, :, j, :].astype(BF16)
@@ -997,12 +1012,14 @@
     for load in loads[1:]:
         load.wait()
     a = ffn[...]
-    dh[...] = (jax.nn.silu(dot(a, dg[...])) * dot(a, du[...])).astype(BF16)
     for core in range(CORES):
         both = dot(a, gu[core])
         eh[:, core * part : (core + 1) * part] = (
             jax.nn.silu(both[:, :part]) * both[:, part:]
         ).astype(BF16)
+    for at in range(0, hid, 2 * LANES):
+        piece = slice(at, at + 2 * LANES)
+        dh[:, piece] = (jax.nn.silu(dot(a, dg[:, piece])) * dot(a, du[:, piece])).astype(BF16)
     blend = jax.nn.sigmoid(jnp.sum(a.astype(F32) * mixw_ref[...], axis=-1, keepdims=True))
     lanes = lax.broadcasted_iota(jnp.int32, (rows_all, route.shape[2]), 1)
     weight = jnp.sum(
@@ -1011,12 +1028,12 @@
         keepdims=True,
     )
     half = CORES * quarter
-    for dy in (1, 0):
+    def project(dy):
         cols = block(flip(y, dy), half)
-        total = blend * dot(dh[...], dd[:, cols]) + weight * dot(eh[...], ed[:, cols])
-        leaving[dy] = total.astype(BF16)
-        if not dy:
-            kept[...] = total
+        sparse = weight * dot(eh[...], ed[:, cols])
+        return sparse + blend * dot(dh[...], dd[:, cols])
+
+    leaving[1] = project(1).astype(BF16)
 
     def leave(i, core, step):
         dx, dy = around[step]
@@ -1042,6 +1059,10 @@
 
     order = range(turns - 1, -1, -1)
     for dy in (1, 0):
+        if not dy:
+            total = project(0)
+            leaving[0] = total.astype(BF16)
+            kept[...] = total
         steps = [step for step in range(len(around)) if around[step][1] == dy]
 
         @pl.when(far)
@@ -1152,6 +1173,15 @@
             @pl.when(jnp.logical_and(z == level, c == core))
             def _(count=count):
                 drained(count)
+
+
+def settle(layer_ref, fresh_ref, layer_out, fresh_out, sem):
+    first = pltpu.make_async_copy(layer_ref, layer_out, sem.at[0])
+    second = pltpu.make_async_copy(fresh_ref, fresh_out, sem.at[1])
+    first.start()
+    second.start()
+    first.wait()
+    second.wait()
 
 
 def near_call(n_ep, n_tp, arrays):
@@ -1274,6 +1304,17 @@
         held(dense_up),
         held(dense_down),
     )
+    layer_out, fresh = pl.pallas_call(
+        settle,
+        out_shape=(
+            jax.ShapeDtypeStruct(layer_out.shape, BF16),
+            jax.ShapeDtypeStruct(fresh.shape, BF16),
+        ),
+        in_specs=[vmem, vmem],
+        out_specs=(hbm, hbm),
+        scratch_shapes=[dma((2,))],
+        compiler_params=pltpu.CompilerParams(vmem_limit_bytes=1024 * 1024),
+    )(layer_out, fresh)
     return layer_out, fresh.reshape(seqs, groups, kv_cache.shape[3])
 
 

time: 28.6 us -> 27.7 us (0.969)
  local copies, waits for them, and re-layouts: 1.21 us -> 0 us
  Pallas kernels: 26.6 us -> 26.9 us
    unnamed x2 -> x0, local copies, waits for them, and re-layouts: 1.21 us -> none
    pallas_call x0 -> x1, Pallas kernels: none -> 0.63 us  [near_call(): pl.pallas_call(settle, out_shape=(jax.ShapeDtypeStruct(layer_out.shape, B...]
    pallas_call x1, Pallas kernels: 26.6 us -> 26.3 us  [near_call(): pl.pallas_call(functools.partial(near_kernel, n_ep, n_tp), out_shape=(jax...]
where the time goes in v4:
time: 27.7 us; the launch traced here: 27.6 us
  Pallas kernels  26.9 us (97%)
  between operations  0.65 us (2%)
    pallas_call x1, Pallas kernels, near_call(): pl.pallas_call(functools.partial(near_kernel, n_ep, n_tp), out_shape=(jax...  26.3 us
    pallas_call x1, Pallas kernels, near_call(): pl.pallas_call(settle, out_shape=(jax.ShapeDtypeStruct(layer_out.shape, B...  0.63 us

profile of v4, /device:TPU:0, one launch (start us, length us, event | category | flops | bytes accessed | tf_op | source)
XLA Modules:
  0.0 27.6 jit_solution(3252493820153855632)
XLA Ops:
  0.6 26.3 %shard_map.203 = (bf16[16,512]{1,0:T(8,128)(2,1)S(1)}, bf16[16,256]{1,0:T(8,128)(2,1)S(1)}) custom-call(s32[16]{0:T(128)} %lengths_hbm.1, f32[4]{0:T(128)} %lam_hbm.1, bf16[16,2048]{1,0:T(8,128)(2,1)} %resid_hbm.1, f32[1,2048]{1,0:T(1,128)} %bitcast.7, f32[1,128]{1,0:T(1,128)} %bitcast.12, f32[1,2048]{1,0:T(1,128)} %bitcast.8, f32[1,2048]{1,0:T(1,128)} %bitcast.9, ...), custom_call_target="tpu_custom_call" | custom-call | tf_op jit(solution)/shard_map/pallas_call | solution.py:1226
  26.9 0.6 %shard_map.204 = (bf16[16,512]{1,0:T(8,128)(2,1)}, bf16[16,256]{1,0:T(8,128)(2,1)}) custom-call(bf16[16,512]{1,0:T(8,128)(2,1)S(1)} %get-tuple-element.6.layer_ref, bf16[16,256]{1,0:T(8,128)(2,1)S(1)} %get-tuple-element.7.fresh_ref), custom_call_target="tpu_custom_call" | custom-call | tf_op jit(solution)/shard_map/pallas_call | solution.py:1307

commit v5 on v4

--- a/solution.py
+++ b/solution.py
@@ -533,6 +533,10 @@
         each(n_ep, gone)
 
 
+def keeps(plane):
+    return (plane + 1) % CORES
+
+
 def near_kernel(
     n_ep,
     n_tp,
@@ -612,8 +616,8 @@
     x = e % INNER
     y = t // CORES
     c = t % CORES
-    keeper = z % CORES
-    odd = (c + z) % CORES
+    keeper = keeps(z)
+    odd = (c + keeper) % CORES
     turns = planes // CORES
     seqs, width = resid_ref.shape
     quarter = out_ref.shape[1]
@@ -940,7 +944,7 @@
             where,
             chunk_send.at[0],
             group_recv.at[plane // CORES, dx],
-            (z * INNER + flip(x, dx), flip(y, dy) * CORES + plane % CORES),
+            (z * INNER + flip(x, dx), flip(y, dy) * CORES + keeps(plane)),
         )
 
     def hand_over(plane, core):
@@ -960,11 +964,11 @@
                     arrived(plane, core)
                     for step in range(len(around)):
                         forward(plane, core, step).start()
-                    if plane % CORES != RELAY:
+                    if keeps(plane) != RELAY:
                         hand_over(plane, core).start()
 
     def normalise(i):
-        plane = CORES * i + c
+        plane = CORES * i + keeps(c)
 
         @pl.when(plane == z)
         def _():
@@ -1035,15 +1039,29 @@
 
     leaving[1] = project(1).astype(BF16)
 
+    def own_plane(i):
+        return jnp.logical_and(odd == 0, i == 0)
+
     def leave(i, core, step):
         dx, dy = around[step]
         where = spot(plane_of(i), flip(x, dx))
+        summer = jnp.where(own_plane(i), c, RELAY)
         return remote(
             leaving.at[dy, block(where, seqs), pl.ds(core * quarter, quarter)],
-            plane_in.at[i, core, step],
+            plane_in.at[c, i, core, step],
             chunk_send.at[0],
-            plane_recv.at[i, core],
-            (z * INNER + flip(x, dx), flip(y, dy) * CORES + c),
+            plane_recv.at[c, i, core],
+            (z * INNER + flip(x, dx), flip(y, dy) * CORES + summer),
+        )
+
+    def pass_over(i, core):
+        where = spot(plane_of(i), x)
+        return remote(
+            leaving.at[0, block(where, seqs), pl.ds(core * quarter, quarter)],
+            plane_in.at[c, i, core, len(around)],
+            chunk_send.at[0],
+            plane_recv.at[c, i, core],
+            (e, mate),
         )
 
     def leap(core, step):
@@ -1077,22 +1095,27 @@
                 for core in range(CORES):
                     for step in steps:
                         leave(i, core, step).start()
+                if not dy:
+
+                    @pl.when(jnp.logical_and(c != RELAY, jnp.logical_not(own_plane(i))))
+                    def _():
+                        for core in range(CORES):
+                            pass_over(i, core).start()
 
             if i == last:
                 pl.when(jnp.logical_not(far))(depart)
             else:
                 depart()
 
-    def own_plane(i):
-        return jnp.logical_and(odd == 0, i == 0)
-
-    def climb(i, core):
+    def climb(lane, i, core):
+        skew = (lane + keeper) % CORES
+        level = flip(z + skew * (1 - 2 * (z % 2)), 2 * i)
         return remote(
-            column_out.at[i, core],
-            column_in.at[odd + 2 * i],
+            column_out.at[lane, i, core],
+            column_in.at[skew + 2 * i],
             chunk_send.at[0],
             column_recv.at[0],
-            (plane_of(i) * INNER + x, y * CORES + core),
+            (level * INNER + x, y * CORES + core),
         )
 
     def stays(i, core):
@@ -1101,24 +1124,48 @@
     def rise(i):
         for core in range(CORES):
             gathered = kept[block(spot(plane_of(i), x), seqs), core * quarter : (core + 1) * quarter]
-            came = plane_in.at[i, core]
-            remote(came, came, chunk_send.at[0], plane_recv.at[i, core], (e, t)).wait_recv()
+            came = plane_in.at[c, i, core, pl.ds(0, len(around))]
+            remote(came, came, chunk_send.at[0], plane_recv.at[c, i, core], (e, t)).wait_recv()
             for step in range(len(around)):
-                gathered = gathered + plane_in[i, core, step].astype(F32)
-            column_out[i, core] = gathered.astype(BF16)
+                gathered = gathered + plane_in[c, i, core, step].astype(F32)
+            column_out[c, i, core] = gathered.astype(BF16)
 
             @pl.when(jnp.logical_not(stays(i, core)))
             def _(i=i, core=core):
-                climb(i, core).start()
+                climb(c, i, core).start()
+
+    low = 1 - RELAY
+
+    def lift(i):
+        for core in range(CORES):
+            came = plane_in.at[low, i, core]
+            remote(came, came, chunk_send.at[0], plane_recv.at[low, i, core], (e, t)).wait_recv()
+            gathered = plane_in[low, i, core, 0].astype(F32)
+            for step in range(1, len(around) + 1):
+                gathered = gathered + plane_in[low, i, core, step].astype(F32)
+            column_out[low, i, core] = gathered.astype(BF16)
+            climb(low, i, core).start()
 
     for i in order:
+        sums = jnp.logical_or(c == RELAY, own_plane(i))
         if i == last:
-
-            @pl.when(jnp.logical_not(far))
-            def _(i=i):
-                rise(i)
-        else:
+            sums = jnp.logical_and(sums, jnp.logical_not(far))
+
+        @pl.when(sums)
+        def _(i=i):
             rise(i)
+
+    slant = (low + keeper) % CORES == 1
+    for i in order:
+        theirs = c == RELAY
+        if i == 0:
+            theirs = jnp.logical_and(theirs, slant)
+        if i == last:
+            theirs = jnp.logical_and(theirs, jnp.logical_not(jnp.logical_and(edge, slant)))
+
+        @pl.when(theirs)
+        def _(i=i):
+            lift(i)
 
     def took(start, stop):
         where = column_in.at[pl.ds(start, stop - start)]
@@ -1126,7 +1173,7 @@
 
     @pl.when(odd == 0)
     def _():
-        column_in[0] = column_out[0, c]
+        column_in[0] = column_out[c, 0, c]
 
     def finish(stop):
         for parity in range(2):
@@ -1165,10 +1212,16 @@
         for core in range(CORES):
             count = planes - 1 + hops + turns * CORES * (hops + 1)
             count += hops if level == planes - 1 else 0
-            count += 1 if (level + core) % CORES else -1
+            count += 1 if core != keeps(level) else -1
+            if core == RELAY:
+                skew = (1 - RELAY + keeps(level)) % CORES
+                lower = [level ^ skew ^ (CORES * i) for i in range(turns)]
+                count += CORES * sum(
+                    plane != level and abs(plane - level) != planes - 1 for plane in lower
+                )
             for plane in range(planes) if core == RELAY else ():
                 if plane != level and plane - level != planes - 1:
-                    count += CORES * (hops + (plane % CORES != RELAY))
+                    count += CORES * (hops + (keeps(plane) != RELAY))
 
             @pl.when(jnp.logical_and(z == level, c == core))
             def _(count=count):
@@ -1263,8 +1316,8 @@
             pltpu.VMEM((rows, hid), BF16),
             pltpu.VMEM((2, rows, CORES * quarter), BF16),
             pltpu.VMEM((rows, CORES * quarter), F32),
-            pltpu.VMEM((turns, CORES, 3, seqs, quarter), BF16),
-            pltpu.VMEM((turns, CORES, seqs, quarter), BF16),
+            pltpu.VMEM((CORES, turns, CORES, 4, seqs, quarter), BF16),
+            pltpu.VMEM((CORES, turns, CORES, seqs, quarter), BF16),
             pltpu.VMEM((n_ep // INNER + 3, seqs, quarter), BF16),
             dma((Q_CHUNKS + CACHE_CHUNKS + 4,)),
             dma((1,)),
@@ -1276,7 +1329,7 @@
             dma((1,)),
             dma((n_ep // INNER, CORES)),
             dma((turns, INNER)),
-            dma((turns, CORES)),
+            dma((CORES, turns, CORES)),
             dma((1,)),
         ],
         compiler_params=pltpu.CompilerParams(

time: 27.7 us -> 26.6 us (0.960)
  the two profiles are of different devices: /device:TPU:0 before, /device:TPU:9 now
where the time goes in v5:
time: 26.6 us; the launch traced here: 26.4 us
  Pallas kernels  25.8 us (97%)
  between operations  0.65 us (2%)
    pallas_call x1, Pallas kernels, near_call(): pl.pallas_call(functools.partial(near_kernel, n_ep, n_tp), out_shape=(jax...  25.1 us
    pallas_call x1, Pallas kernels, near_call(): pl.pallas_call(settle, out_shape=(jax.ShapeDtypeStruct(layer_out.shape, B...  0.63 us

profile of v5, /device:TPU:9, one launch (start us, length us, event | category | flops | bytes accessed | tf_op | source)
XLA Modules:
  0.0 26.4 jit_solution(293840947253824304)
XLA Ops:
  0.6 25.1 %shard_map.203 = (bf16[16,512]{1,0:T(8,128)(2,1)S(1)}, bf16[16,256]{1,0:T(8,128)(2,1)S(1)}) custom-call(s32[16]{0:T(128)} %lengths_hbm.1, f32[4]{0:T(128)} %lam_hbm.1, bf16[16,2048]{1,0:T(8,128)(2,1)} %resid_hbm.1, f32[1,2048]{1,0:T(1,128)} %bitcast.7, f32[1,128]{1,0:T(1,128)} %bitcast.12, f32[1,2048]{1,0:T(1,128)} %bitcast.8, f32[1,2048]{1,0:T(1,128)} %bitcast.9, ...), custom_call_target="tpu_custom_call" | custom-call | tf_op jit(solution)/shard_map/pallas_call | solution.py:1279
  25.8 0.6 %shard_map.204 = (bf16[16,512]{1,0:T(8,128)(2,1)}, bf16[16,256]{1,0:T(8,128)(2,1)}) custom-call(bf16[16,512]{1,0:T(8,128)(2,1)S(1)} %get-tuple-element.6.layer_ref, bf16[16,256]{1,0:T(8,128)(2,1)S(1)} %get-tuple-element.7.fresh_ref), custom_call_target="tpu_custom_call" | custom-call | tf_op jit(solution)/shard_map/pallas_call | solution.py:1360

commit v6 on v5

--- a/solution.py
+++ b/solution.py
@@ -535,6 +535,16 @@
 
 def keeps(plane):
     return (plane + 1) % CORES
+
+
+def tells(planes, me, you):
+    z, x, y, c = me
+    level, inner, side, core = you
+    other = (z != level) | (x != inner) | (y != side) | (c != core)
+    column = (c == RELAY) & (x == inner) & (y == side)
+    lane = (y == side) & (c == core)
+    far = (z == 0) & (level == planes - 1) & (c == keeps(planes - 1))
+    return other & ((z == level) | column | lane | far)
 
 
 def near_kernel(
@@ -648,11 +658,25 @@
 
     barrier = pltpu.get_barrier_semaphore()
     for index in range(n_ep * n_tp):
-        where = (index // n_tp, index % n_tp)
-
-        @pl.when(jnp.logical_or(where[0] != e, where[1] != t))
+        there = (index // n_tp // INNER, index // n_tp % INNER, index % n_tp // CORES, index % CORES)
+
+        @pl.when(tells(planes, (z, x, y, c), there))
         def _():
-            pl.semaphore_signal(barrier, inc=1, device_id=where, device_id_type=MESH)
+            pl.semaphore_signal(
+                barrier, inc=1, device_id=(index // n_tp, index % n_tp), device_id_type=MESH
+            )
+
+    told = 0
+    for level in range(planes):
+        for core in range(CORES):
+            count = sum(
+                tells(planes, (i, j, k, m), (level, 0, 0, core))
+                for i in range(planes)
+                for j in range(INNER)
+                for k in range(n_tp // CORES)
+                for m in range(CORES)
+            )
+            told = jnp.where((z == level) & (c == core), count, told)
 
     for load in first_loads:
         load.wait()
@@ -834,7 +858,7 @@
             (e, flip(t, mask)),
         )
 
-    pl.semaphore_wait(barrier, n_ep * n_tp - 1)
+    pl.semaphore_wait(barrier, told)
     for mask in range(n_tp - 1, 0, -1):
         heads_copy(mask).start()
 

time: 26.6 us -> 26 us (0.977)
  the two profiles are of different devices: /device:TPU:9 before, /device:TPU:0 now
where the time goes in v6:
time: 26 us; the launch traced here: 25.6 us
  Pallas kernels  24.9 us (96%)
  between operations  0.65 us (2%)
    pallas_call x1, Pallas kernels, near_call(): pl.pallas_call(functools.partial(near_kernel, n_ep, n_tp), out_shape=(jax...  24.3 us
    pallas_call x1, Pallas kernels, near_call(): pl.pallas_call(settle, out_shape=(jax.ShapeDtypeStruct(layer_out.shape, B...  0.63 us

profile of v6, /device:TPU:0, one launch (start us, length us, event | category | flops | bytes accessed | tf_op | source)
XLA Modules:
  0.0 25.6 jit_solution(15639360156101065110)
XLA Ops:
  0.6 24.3 %shard_map.203 = (bf16[16,512]{1,0:T(8,128)(2,1)S(1)}, bf16[16,256]{1,0:T(8,128)(2,1)S(1)}) custom-call(s32[16]{0:T(128)} %lengths_hbm.1, f32[4]{0:T(128)} %lam_hbm.1, bf16[16,2048]{1,0:T(8,128)(2,1)} %resid_hbm.1, f32[1,2048]{1,0:T(1,128)} %bitcast.7, f32[1,128]{1,0:T(1,128)} %bitcast.12, f32[1,2048]{1,0:T(1,128)} %bitcast.8, f32[1,2048]{1,0:T(1,128)} %bitcast.9, ...), custom_call_target="tpu_custom_call" | custom-call | tf_op jit(solution)/shard_map/pallas_call | solution.py:1303
  25.0 0.6 %shard_map.204 = (bf16[16,512]{1,0:T(8,128)(2,1)}, bf16[16,256]{1,0:T(8,128)(2,1)}) custom-call(bf16[16,512]{1,0:T(8,128)(2,1)S(1)} %get-tuple-element.6.layer_ref, bf16[16,256]{1,0:T(8,128)(2,1)S(1)} %get-tuple-element.7.fresh_ref), custom_call_target="tpu_custom_call" | custom-call | tf_op jit(solution)/shard_map/pallas_call | solution.py:1384

commit v7 on v6

--- a/solution.py
+++ b/solution.py
@@ -859,8 +859,16 @@
         )
 
     pl.semaphore_wait(barrier, told)
-    for mask in range(n_tp - 1, 0, -1):
-        heads_copy(mask).start()
+    for core in range(CORES):
+        skew = (c + core) % CORES
+        remote(
+            heads_ref,
+            heads_all.at[CORES - 1 + skew],
+            heads_send.at[0],
+            heads_recv.at[1],
+            (e, flip(y, 1) * CORES + core),
+        ).start()
+    heads_copy(1).start()
 
     for load in e_loads:
         load.wait()
@@ -977,14 +985,14 @@
 
     @pl.when(c == RELAY)
     def _():
-        for plane in range(planes):
+        for plane in sorted(range(planes), key=lambda plane: keeps(plane) != RELAY):
             passes = plane != z
             if plane == planes - 1:
                 passes = jnp.logical_and(passes, z != 0)
 
             @pl.when(passes)
             def _(plane=plane):
-                for core in range(CORES):
+                for core in (RELAY, 1 - RELAY):
                     arrived(plane, core)
                     for step in range(len(around)):
                         forward(plane, core, step).start()

time: 26 us -> 25.3 us (0.973)
  the two profiles are of different devices: /device:TPU:0 before, /device:TPU:1 now
where the time goes in v7:
time: 25.3 us; the launch traced here: 25.1 us
  Pallas kernels  24.5 us (97%)
  between operations  0.65 us (3%)
    pallas_call x1, Pallas kernels, near_call(): pl.pallas_call(functools.partial(near_kernel, n_ep, n_tp), out_shape=(jax...  23.9 us
    pallas_call x1, Pallas kernels, near_call(): pl.pallas_call(settle, out_shape=(jax.ShapeDtypeStruct(layer_out.shape, B...  0.63 us

profile of v7, /device:TPU:1, one launch (start us, length us, event | category | flops | bytes accessed | tf_op | source)
XLA Modules:
  0.0 25.1 jit_solution(11326761753040196185)
XLA Ops:
  0.6 23.9 %shard_map.203 = (bf16[16,512]{1,0:T(8,128)(2,1)S(1)}, bf16[16,256]{1,0:T(8,128)(2,1)S(1)}) custom-call(s32[16]{0:T(128)} %lengths_hbm.1, f32[4]{0:T(128)} %lam_hbm.1, bf16[16,2048]{1,0:T(8,128)(2,1)} %resid_hbm.1, f32[1,2048]{1,0:T(1,128)} %bitcast.7, f32[1,128]{1,0:T(1,128)} %bitcast.12, f32[1,2048]{1,0:T(1,128)} %bitcast.8, f32[1,2048]{1,0:T(1,128)} %bitcast.9, ...), custom_call_target="tpu_custom_call" | custom-call | tf_op jit(solution)/shard_map/pallas_call | solution.py:1311
  24.5 0.6 %shard_map.204 = (bf16[16,512]{1,0:T(8,128)(2,1)}, bf16[16,256]{1,0:T(8,128)(2,1)}) custom-call(bf16[16,512]{1,0:T(8,128)(2,1)S(1)} %get-tuple-element.6.layer_ref, bf16[16,256]{1,0:T(8,128)(2,1)S(1)} %get-tuple-element.7.fresh_ref), custom_call_target="tpu_custom_call" | custom-call | tf_op jit(solution)/shard_map/pallas_call | solution.py:1392

commit v8 on v7

--- a/solution.py
+++ b/solution.py
@@ -870,10 +870,6 @@
         ).start()
     heads_copy(1).start()
 
-    for load in e_loads:
-        load.wait()
-    push(0).start()
-    push(1).start()
 
     lane = lax.broadcasted_iota(jnp.int32, (seqs, route.shape[2]), 1)
     table = jnp.zeros((seqs, route.shape[2]), F32)
@@ -958,6 +954,11 @@
     @pl.when(odd == 0)
     def _():
         stream[block(e, seqs), own_cols] = own_stream
+
+    for load in e_loads:
+        load.wait()
+    push(0).start()
+    push(1).start()
 
     near = z + odd * (1 - 2 * (z % 2))
 

time: 25.3 us -> 25.3 us (level)
  no operation moved by 1% of the time
where the time goes in v8:
time: 25.3 us; the launch traced here: 25.1 us
  Pallas kernels  24.5 us (97%)
  between operations  0.65 us (3%)
    pallas_call x1, Pallas kernels, near_call(): pl.pallas_call(functools.partial(near_kernel, n_ep, n_tp), out_shape=(jax...  23.9 us
    pallas_call x1, Pallas kernels, near_call(): pl.pallas_call(settle, out_shape=(jax.ShapeDtypeStruct(layer_out.shape, B...  0.63 us

profile of v8, /device:TPU:1, one launch (start us, length us, event | category | flops | bytes accessed | tf_op | source)
XLA Modules:
  0.0 25.1 jit_solution(9201630483332556104)
XLA Ops:
  0.6 23.9 %shard_map.203 = (bf16[16,512]{1,0:T(8,128)(2,1)S(1)}, bf16[16,256]{1,0:T(8,128)(2,1)S(1)}) custom-call(s32[16]{0:T(128)} %lengths_hbm.1, f32[4]{0:T(128)} %lam_hbm.1, bf16[16,2048]{1,0:T(8,128)(2,1)} %resid_hbm.1, f32[1,2048]{1,0:T(1,128)} %bitcast.7, f32[1,128]{1,0:T(1,128)} %bitcast.12, f32[1,2048]{1,0:T(1,128)} %bitcast.8, f32[1,2048]{1,0:T(1,128)} %bitcast.9, ...), custom_call_target="tpu_custom_call" | custom-call | tf_op jit(solution)/shard_map/pallas_call | solution.py:1312
  24.5 0.6 %shard_map.204 = (bf16[16,512]{1,0:T(8,128)(2,1)}, bf16[16,256]{1,0:T(8,128)(2,1)}) custom-call(bf16[16,512]{1,0:T(8,128)(2,1)S(1)} %get-tuple-element.6.layer_ref, bf16[16,256]{1,0:T(8,128)(2,1)S(1)} %get-tuple-element.7.fresh_ref), custom_call_target="tpu_custom_call" | custom-call | tf_op jit(solution)/shard_map/pallas_call | solution.py:1393
